TPU v7x, 512 devices: a whole 4x4x16 slice. The times are simulated.
512 devices in a mesh: sp: 32 (over z, core), tp: 16 (over y, x).
Axes of the slice: x: 4, y: 4, z: 16, core: 2. Of those that a mesh axis runs over, the one named last changes fastest.
Arguments:
- stream: bfloat16 [12288, 2048], P('sp'), may hold values from -6 to 6
- inner_act: bfloat16 [12288, 4096], P('sp', 'tp'), may hold values from -6 to 6
- gate_act: bfloat16 [12288, 4096], P('sp', 'tp'), may hold values from -6 to 6
- state_write: bfloat16 [12288, 16, 128], P('sp', 'tp'), may hold values from -6 to 6
- state_read: bfloat16 [12288, 16, 128], P('sp', 'tp'), may hold values from -6 to 6
- step_raw: bfloat16 [12288, 64], P('sp', 'tp'), may hold values from -4.6 to 4.1
- conv_inner: bfloat16 [4, 4096], P(None, 'tp'), may hold values from -3 to 3
- conv_write: bfloat16 [4, 16, 128], P(None, 'tp'), may hold values from -3 to 3
- conv_read: bfloat16 [4, 16, 128], P(None, 'tp'), may hold values from -3 to 3
- step_bias: float32 [64], P('tp'), may hold values from -0.5 to 0.5
- decay_log: float32 [64], P('tp'), may hold values from -13 to -2.52, as said below
- inner_gain: float32 [4096], P('tp'), may hold values from 0.1 to 1.9
- out_weight: bfloat16 [4096, 2048], P('tp'), may hold values from -0.09375 to 0.09375
- ffn_gain: float32 [2048], replicated, may hold values from 0.1 to 1.9
- expert_ids: int32 [12288, 2], P('sp'), may hold values from 0 to 31, all different within a row; in each aligned block of 384 rows (0 to 383, 384 to 767, ...) at most 48 rows name the same one
- expert_weights: float32 [12288, 2], P('sp'), may hold values from 0.1 to 1
- expert_gate: bfloat16 [32, 2048, 1024], P('sp', None, 'tp'), may hold values from -0.125 to 0.125
- expert_up: bfloat16 [32, 2048, 1024], P('sp', None, 'tp'), may hold values from -0.125 to 0.125
- expert_down: bfloat16 [32, 1024, 2048], P('sp', None, 'tp'), may hold values from -0.1875 to 0.1875
Outputs:
- layer_out: bfloat16 [12288, 2048], P('sp', 'tp')
Inputs may be any that keep to these rules, and one draw needn't show every extreme that they name: The logarithm of a per-position decay rate: exp(decay_log) lies between 0.1 / 12288 and 0.08. `expert_ids`: each row names 2 different experts. Among the rows of one index of sp (384 tokens) no expert is named more than 48 times, a bound that some block reaches there.
All inputs are finite; a program needn't handle non-finite values.
Results may differ from a plain program's by a relative error of at most 0.014.
Values may be sent and summed in bfloat16 or wider, within the bound.
A program may use at most 64 MiB of HBM per device.

v0:
```python
import functools

import jax
import jax.numpy as jnp
from jax import lax
from jax.sharding import Mesh
from jax.sharding import PartitionSpec as P

BLOCK = 64
TOPK = 2
CAP = 48
SP = ("sp_0", "sp_1")
TP = ("tp_0", "tp_1")


HIGH = lax.Precision.HIGHEST
EPS = 1e-06


def from_behind(value, axis, steps):
    count = lax.axis_size(axis)
    first, last = (max(0, -steps), min(count, count - steps))
    return lax.ppermute(value, axis, [(source, source + steps) for source in range(first, last)])


def nothing_yet(value, identity):
    return jax.tree.map(
        lambda a, e: jnp.broadcast_to(jnp.asarray(e, a.dtype), a.shape), value, identity
    )


def entering_2(value, axes, combine, identity):
    before = start = nothing_yet(value, identity)
    running = value
    for axis in reversed(axes):
        size, mine = (lax.axis_size(axis), lax.axis_index(axis))
        pieces = jax.tree.map(
            lambda part, kind: lax.all_gather(part.astype(kind), axis),
            running,
            (jnp.bfloat16, jnp.bfloat16),
        )
        inside, running = (start, start)
        for k in range(size):
            passed = k < mine
            running = combine(
                running, jax.tree.map(lambda part, own: part[k].astype(own.dtype), pieces, value)
            )
            inside = jax.tree.map(lambda new, old: jnp.where(passed, new, old), running, inside)
        before = combine(inside, before)
    return before


def split_up(value, dim, size):
    before, after = (value.shape[:dim], value.shape[dim + 1 :])
    return jnp.moveaxis(value.reshape(*before, size, -1, *after), dim, 0)


def sent_and_summed(value, axis, dim):
    tiles = split_up(value, dim, lax.axis_size(axis))
    arrived = lax.all_to_all(tiles, axis, split_axis=0, concat_axis=0, tiled=True)
    return arrived.astype(jnp.float32).sum(axis=0)


def one_axis_at_a_time(value, axes):
    return functools.reduce(lax.psum, axes, value)


def whole_of(value, axes, dim):
    whole = value
    for number in range(len(axes) - 1, -1, -1):
        whole = lax.all_gather(whole, axes[number], axis=dim, tiled=True)
    return whole


def conv_silu(padded, weights, length):
    running = jnp.zeros((length, padded.shape[1]), jnp.float32)
    for offset in range(weights.shape[0]):
        running = running + weights[offset][None, :] * padded[offset : offset + length]
    return jax.nn.silu(running)


def block_terms(values, step_len, decay_rate, writes, reads, block_len):
    blocks = values.shape[0] // block_len
    groups, per_group, head_dim = (values.shape[1], values.shape[2], values.shape[3])
    state_dim = writes.shape[2]
    value_blk = values.reshape(blocks, block_len, groups, per_group, head_dim)
    step_blk = step_len.reshape(blocks, block_len, groups, per_group)
    write_blk = writes.reshape(blocks, block_len, groups, state_dim)
    read_blk = reads.reshape(blocks, block_len, groups, state_dim)
    cumul = jnp.cumsum(step_blk * decay_rate, axis=1)
    causal = jnp.tril(jnp.ones((block_len, block_len), dtype=bool))[None, :, :, None, None]
    spread = cumul[:, :, None] - cumul[:, None, :]
    within = jnp.where(causal, jnp.exp(jnp.where(causal, spread, 0.0)), 0.0)
    intersect = jnp.einsum("clgn,csgn->clsg", read_blk, write_blk, precision=HIGH)
    mixing = intersect[..., None] * within * step_blk[:, None]
    inside = jnp.einsum("clsgh,csghp->clghp", mixing, value_blk, precision=HIGH)
    to_end = jnp.exp(cumul[:, -1:] - cumul) * step_blk
    block_state = jnp.einsum(
        "clgn,clghp->cghpn", write_blk, to_end[..., None] * value_blk, precision=HIGH
    )
    block_decay = jnp.exp(cumul[:, -1])

    def advance(carried, inputs):
        state_here, decay_here = inputs
        return (carried * decay_here[..., None, None] + state_here, carried)

    initial = jnp.zeros(block_state.shape[1:], jnp.float32)
    closing, entering = lax.scan(advance, initial, (block_state, block_decay))
    return (inside, entering, cumul, read_blk, closing)


def chain(earlier_part, later_part):
    return (
        earlier_part[0] * later_part[0],
        earlier_part[1] * later_part[0][..., None, None] + later_part[1],
    )


def per_device(
    stream,
    inner_act,
    gate_act,
    state_write,
    state_read,
    step_raw,
    conv_inner,
    conv_write,
    conv_read,
    step_bias,
    decay_log,
    inner_gain,
    out_weight,
    ffn_gain,
    expert_ids,
    expert_weights,
    expert_gate,
    expert_up,
    expert_down,
):
    length = inner_act.shape[0]
    heads_here = step_raw.shape[1]
    groups_here = state_write.shape[1]
    state_dim = state_write.shape[2]
    inner_width = inner_act.shape[1]
    head_dim = inner_width // heads_here
    per_group = heads_here // groups_here
    write_width = groups_here * state_dim
    joined = jnp.concatenate(
        [
            inner_act,
            state_write.reshape(length, write_width),
            state_read.reshape(length, write_width),
        ],
        axis=1,
    )
    kernel = jnp.concatenate(
        [conv_inner, conv_write.reshape(-1, write_width), conv_read.reshape(-1, write_width)],
        axis=1,
    ).astype(jnp.float32)
    lag_rows = kernel.shape[0] - 1
    earlier = from_behind(joined[length - lag_rows :], SP, 1)
    padded = jnp.concatenate([earlier, joined], axis=0).astype(jnp.float32)
    conv_out = conv_silu(padded, kernel, length)
    values = conv_out[:, :inner_width].reshape(length, groups_here, per_group, head_dim)
    writes = conv_out[:, inner_width : inner_width + write_width].reshape(
        length, groups_here, state_dim
    )
    reads = conv_out[:, inner_width + write_width :].reshape(length, groups_here, state_dim)
    step_len = jax.nn.softplus(step_raw.astype(jnp.float32) + step_bias[None, :]).reshape(
        length, groups_here, per_group
    )
    decay_rate = (-jnp.exp(decay_log)).reshape(groups_here, per_group)
    inside, entering, cumul, read_blk, closing = block_terms(
        values, step_len, decay_rate, writes, reads, BLOCK
    )
    block_sums = cumul[:, -1]
    device_decay = jnp.exp(jnp.sum(block_sums, axis=0))
    unused_decay, arriving = entering_2(
        (device_decay, closing), SP, chain, (jnp.ones_like(device_decay), jnp.zeros_like(closing))
    )
    before = jnp.exp(jnp.cumsum(block_sums, axis=0) - block_sums)
    entering = entering + arriving[None] * before[..., None, None]
    outside = (
        jnp.einsum("clgn,cghpn->clghp", read_blk, entering, precision=HIGH)
        * jnp.exp(cumul)[..., None]
    )
    gated = (inside + outside).reshape(length, inner_width) * jax.nn.silu(
        gate_act.astype(jnp.float32)
    )
    per_head = gated.reshape(length, heads_here, head_dim)
    per_head = per_head * lax.rsqrt(jnp.mean(per_head * per_head, axis=-1, keepdims=True) + EPS)
    mixed_inner = (per_head.reshape(length, inner_width) * inner_gain[None, :]).astype(jnp.bfloat16)
    partial_value = jnp.dot(mixed_inner, out_weight, preferred_element_type=jnp.float32)
    full_width = partial_value.shape[1]
    local_experts = expert_gate.shape[0]
    expert_count = local_experts * lax.axis_size(SP)
    flat_ids = expert_ids.reshape(-1)
    onehot = (flat_ids[:, None] == jnp.arange(expert_count, dtype=jnp.int32)[None, :]).astype(
        jnp.int32
    )
    earlier_count = jnp.cumsum(onehot, axis=0) - onehot
    slot_of = jnp.sum(earlier_count * onehot, axis=1)
    target = flat_ids * CAP + slot_of
    token_of = jnp.arange(flat_ids.shape[0], dtype=jnp.int32) // TOPK
    slot_table = jnp.full((expert_count * CAP,), length, jnp.int32).at[target].set(token_of)
    slot_table = slot_table.reshape(expert_count, CAP)
    out_width = expert_down.shape[2]
    own_start = lax.axis_index(TP) * out_width
    projected = sent_and_summed(partial_value.astype(jnp.bfloat16), TP, 1)
    kept = lax.dynamic_slice_in_dim(stream, own_start, out_width, 1).astype(jnp.float32) + projected
    square_total = one_axis_at_a_time(jnp.sum(kept * kept, axis=1), TP)
    gain_share = lax.dynamic_slice_in_dim(ffn_gain, own_start, out_width, 0)
    scale_rows = lax.rsqrt(square_total / full_width + EPS)
    normed = (kept * scale_rows[:, None] * gain_share[None, :]).astype(jnp.bfloat16)
    padded_rows = jnp.concatenate([normed, jnp.zeros((1, out_width), jnp.bfloat16)], axis=0)
    outgoing = padded_rows[slot_table]
    arrived = lax.all_to_all(outgoing, SP, split_axis=0, concat_axis=0, tiled=True)
    ff_here = expert_gate.shape[2]
    piece_cols = lax.all_gather(arrived, TP, axis=2, tiled=True)
    width_here = piece_cols.shape[2]
    grouped = piece_cols.reshape(-1, local_experts, CAP, width_here)
    gate_add = jnp.einsum(
        "secd,edf->secf", grouped, expert_gate, preferred_element_type=jnp.float32
    )
    up_add = jnp.einsum("secd,edf->secf", grouped, expert_up, preferred_element_type=jnp.float32)
    hidden_all = (jax.nn.silu(gate_add) * up_add).astype(jnp.bfloat16).reshape(-1, CAP, ff_here)
    piece_rows = whole_of(hidden_all, TP, 2)
    grouped = piece_rows.reshape(-1, local_experts, piece_rows.shape[1], piece_rows.shape[2])
    summed = jnp.einsum("secf,efd->secd", grouped, expert_down, preferred_element_type=jnp.float32)
    returned = lax.all_to_all(
        summed.astype(jnp.bfloat16), SP, split_axis=0, concat_axis=0, tiled=True
    )
    results = returned.reshape(expert_count * CAP, out_width)
    picked = results[target].astype(jnp.float32).reshape(length, TOPK, out_width)
    moe = jnp.sum(picked * expert_weights[:, :, None], axis=1)
    return (kept + moe).astype(jnp.bfloat16)


def solution(mesh):
    finer = Mesh(mesh.devices.reshape(16, 2, 4, 4), ("sp_0", "sp_1", "tp_0", "tp_1"))
    return jax.shard_map(
        per_device,
        mesh=finer,
        in_specs=(
            P(SP, None),
            P(SP, TP),
            P(SP, TP),
            P(SP, TP, None),
            P(SP, TP, None),
            P(SP, TP),
            P(None, TP),
            P(None, TP, None),
            P(None, TP, None),
            P(TP),
            P(TP),
            P(TP),
            P(TP, None),
            P(),
            P(SP, None),
            P(SP, None),
            P(SP, None, TP),
            P(SP, None, TP),
            P(SP, None, TP),
        ),
        out_specs=P(SP, TP),
        check_vma=False,
    )
```

profile of v0, /device:TPU:1, one launch (start us, length us, event | category | flops | bytes accessed | tf_op | source)
XLA Modules:
  0.0 410.0 jit_solution(11340880263056351235)
XLA Ops:
  7.4 4.9 %collective-permute-start = (bf16[3,512]{1,0:T(4,128)(2,1)S(1)}, bf16[3,512]{1,0:T(4,128)(2,1)S(1)}, u32[]{:S(2)}, u32[]{:S(2)}) collective-permute-start(bf16[3,512]{1,0:T(4,128)(2,1)S(1)} %pad_maximum_fusion), channel_id=1, source_target_pairs={{0,16},{16,32},{32,48},{48,64},{64,80},{80,96},{96,112},{112,128},... | collective-permute-start | bytes 9224 | tf_op jit(solution)/shard_map/ppermute | solution.py:23
  17.5 5.3 %all-reduce.1 = bf16[8]{0:T(256)(128)(2,1)S(1)} all-reduce(bf16[8]{0:T(256)(128)(2,1)S(1)} %dynamic-update-slice), channel_id=2, replica_groups=mesh['sp_0'=16,'sp_1'=2,'tp_0'=4,'tp_1'=4] {'sp_1'}, use_global_device_ids=true, to_apply=%add.1 | all-reduce | flops 8 | bytes 32
  28.0 1.4 convolution_bitcast_fusion.3
  29.4 8.5 %while.13 = (s32[]{:T(128)}, f32[1,4,64,128]{3,2,1,0:T(8,128)S(1)}, f32[6,1,4,64,128]{4,3,2,1,0:T(8,128)}, f32[6,1,4]{2,1,0:T(1,128)}, f32[6,1,4,64,128]{4,3,2,1,0:T(8,128)S(1)}, /*index=5*/s32[]{:T(128)}, s32[]{:T(128)}) while((s32[]{:T(128)}, f32[1,4,64,128]{3,2,1,0:T(8,128)S(1)}, f32[6,1,4,64,128]{4,3,2,1,0:T(8,128)}, ...), condition=%wide.region_2.3_spmd.clone, body=%wide.region_1.2_spmd.clone.sunk | while | flops 131075 | bytes 656016 | solution.py:108
  38.0 2.0 all-gather.1
  41.6 1.6 copy.98
  43.5 24.1 %all_gather.28 = bf16[16,1,4]{2,1,0:T(2,128)(2,1)S(1)} all-gather(bf16[1,1,4]{2,1,0:T(2,128)(2,1)} %get-tuple-element.108), channel_id=1, replica_groups=mesh['sp_0'=16,'sp_1'=2,'tp_0'=4,'tp_1'=4] {'sp_0'}, dimensions={0}, use_global_device_ids=true | all-gather | bytes 136 | tf_op jit(solution)/shard_map/all_gather | solution.py:38
  69.9 31.5 %all-gather.8.cloned.1.call-done = bf16[16,1,4,64,128]{4,3,2,1,0:T(8,128)(2,1)} async-done(((bf16[1,1,4,64,128]{4,3,2,1,0:T(8,128)(2,1)}), bf16[16,1,4,64,128]{4,3,2,1,0:T(8,128)(2,1)}) %all-gather.8.cloned.1.call-update) | async-done | bytes 1048592 | tf_op jit(solution)/shard_map/all_gather | solution.py:38
  101.5 1.7 fusion.49
  103.2 1.6 fusion.6
  104.9 1.6 fusion.5
  108.5 1.6 copy.123
  110.1 6.3 %all-to-all-start = ((bf16[16,384,128]{2,1,0:T(8,128)(2,1)}), bf16[16,384,128]{2,1,0:T(8,128)(2,1)S(1)}, u32[]{:S(2)}, u32[]{:S(2)}) async-start(bf16[16,384,128]{2,1,0:T(8,128)(2,1)} %bitcast.250), calls=%async_computation | async-start | bytes 3145728 | tf_op jit(solution)/shard_map/all_to_all | solution.py:60
  117.1 1.7 reduce-window.6
  119.6 3.4 scatter_custom_fusion
  123.9 8.7 %all-to-all-done = bf16[16,384,128]{2,1,0:T(8,128)(2,1)S(1)} async-done(((bf16[16,384,128]{2,1,0:T(8,128)(2,1)}), bf16[16,384,128]{2,1,0:T(8,128)(2,1)S(1)}, u32[]{:S(2)}, u32[]{:S(2)}) %all-to-all-start) | async-done | bytes 1572896 | tf_op jit(solution)/shard_map/all_to_all | solution.py:60
  133.9 8.1 %psum.14 = f32[384]{0:T(512)S(1)} all-reduce(f32[384]{0:T(512)S(1)} %multiply_reduce_fusion), channel_id=1, replica_groups=mesh['sp_0'=16,'sp_1'=2,'tp_0'=4,'tp_1'=4] {'tp_0'}, use_global_device_ids=true, to_apply=%region_8.9 | all-reduce | flops 384 | bytes 3072 | tf_op jit(solution)/shard_map/psum | solution.py:65
  142.1 6.0 %psum.15 = f32[384]{0:T(512)S(1)} all-reduce(f32[384]{0:T(512)S(1)} %psum.14), channel_id=1, replica_groups=mesh['sp_0'=16,'sp_1'=2,'tp_0'=4,'tp_1'=4] {'tp_1'}, use_global_device_ids=true, to_apply=%region_9.10 | all-reduce | flops 384 | bytes 3072 | tf_op jit(solution)/shard_map/psum | solution.py:65
  149.1 3.2 gather_fusion
  152.3 51.1 %all_to_all.15 = bf16[32,48,128]{2,1,0:T(8,128)(2,1)} all-to-all(bf16[32,48,128]{2,1,0:T(8,128)(2,1)S(1)} %bitcast.259), channel_id=1, replica_groups=mesh['sp_0'=16,'sp_1'=2,'tp_0'=4,'tp_1'=4] {'sp_0','sp_1'}, dimensions={0} | all-to-all | bytes 786432 | tf_op jit(solution)/shard_map/all_to_all | solution.py:217
  203.5 69.0 %all-gather.10.cloned.1.call-done = bf16[32,48,2048]{2,1,0:T(8,128)(2,1)} async-done(((bf16[32,48,128]{2,1,0:T(8,128)(2,1)}), bf16[32,48,2048]{2,1,0:T(8,128)(2,1)}) %all-gather.10.cloned.1.call-update) | async-done | bytes 6291472 | tf_op jit(solution)/shard_map/all_gather | solution.py:219
  272.6 4.7 %convolution_bitcast_fusion.1 = f32[32,1,48,64]{3,2,0,1:T(8,128)S(1)} fusion(bf16[32,48,2048]{2,1,0:T(8,128)(2,1)} %all-gather.10.cloned.1.call-done, bf16[1,2048,64]{1,2,0:T(8,128)(2,1)S(1)} %copy-done.11), kind=kOutput, calls=%fused_computation.14 | convolution fusion | flops 402653184 | bytes 6946816 | tf_op jit(solution)/shard_map/secd,edf->secf/dot_general | solution.py:222
  277.4 1.8 fusion.7
  279.2 1.5 copy.107
  280.7 19.4 %all-gather.2 = bf16[32,1,48,256]{2,0,1,3:T(8,128)(2,1)S(1)} all-gather(bf16[32,1,48,64]{2,0,1,3:T(8,128)(2,1)} %copy.107), channel_id=4, replica_groups=mesh['sp_0'=16,'sp_1'=2,'tp_0'=4,'tp_1'=4] {'tp_1'}, dimensions={3}, use_global_device_ids=true | all-gather | bytes 983040 | tf_op jit(solution)/shard_map/all_gather | solution.py:71
  300.1 2.4 copy.108
  302.5 51.2 %all-gather.12.cloned.1.call-done = bf16[32,1,48,1024]{3,2,0,1:T(8,128)(2,1)} async-done(((bf16[32,1,48,256]{3,2,0,1:T(8,128)(2,1)}), bf16[32,1,48,1024]{3,2,0,1:T(8,128)(2,1)}) %all-gather.12.cloned.1.call-update) | async-done | bytes 3145744 | tf_op jit(solution)/shard_map/all_gather | solution.py:71
  353.7 3.6 fusion.11
  357.3 14.4 %all-to-all-start.2 = ((bf16[32,1,48,128]{3,2,1,0:T(8,128)(2,1)}), bf16[32,1,48,128]{3,2,1,0:T(8,128)(2,1)S(1)}, u32[]{:S(2)}, u32[]{:S(2)}) async-start(bf16[32,1,48,128]{3,2,1,0:T(8,128)(2,1)} %fusion.11), calls=%async_computation.2 | async-start | bytes 786432 | tf_op jit(solution)/shard_map/all_to_all | solution.py:230
  371.9 27.6 %all-to-all-done.2 = bf16[32,1,48,128]{3,2,1,0:T(8,128)(2,1)S(1)} async-done(((bf16[32,1,48,128]{3,2,1,0:T(8,128)(2,1)}), bf16[32,1,48,128]{3,2,1,0:T(8,128)(2,1)S(1)}, u32[]{:S(2)}, u32[]{:S(2)}) %all-to-all-start.2) | async-done | bytes 393248 | tf_op jit(solution)/shard_map/all_to_all | solution.py:230
  399.5 1.9 gather_fusion.1
  401.9 1.6 add_convert_fusion
  (127 shorter events, 30.5 us)
Async XLA Ops:
  6.5 101.3 %copy-start = (bf16[256,2048]{1,0:T(8,128)(2,1)S(1)}, bf16[256,2048]{1,0:T(8,128)(2,1)}, u32[]{:S(2)}) copy-start(bf16[256,2048]{1,0:T(8,128)(2,1)} %param.33) | copy-start | bytes 3145732
  6.5 94.9 %all-gather.8.cloned.1.call-start = ((), (), s32[]{:S(2)}) async-start(), calls=%async_computation.3 | async-start | bytes 1114112 | tf_op jit(solution)/shard_map/all_gather | solution.py:38
  7.4 18.1 %collective-permute-start = (bf16[3,512]{1,0:T(4,128)(2,1)S(1)}, bf16[3,512]{1,0:T(4,128)(2,1)S(1)}, u32[]{:S(2)}, u32[]{:S(2)}) collective-permute-start(bf16[3,512]{1,0:T(4,128)(2,1)S(1)} %pad_maximum_fusion), channel_id=1, source_target_pairs={{0,16},{16,32},{32,48},{48,64},{64,80},{80,96},{96,112},{112,128},... | collective-permute-start | bytes 9224 | tf_op jit(solution)/shard_map/ppermute | solution.py:23
  24.8 15.2 %copy-start.6 = (f32[4]{0:T(128)}, f32[4]{0:T(128)S(1)}, u32[]{:S(2)}) copy-start(f32[4]{0:T(128)S(1)} %get-tuple-element.109) | copy-start | bytes 52
  28.0 12.0 %copy-start.8 = (f32[4]{0:T(128)S(1)}, f32[4]{0:T(128)}, u32[]{:S(2)}) copy-start(f32[4]{0:T(128)} %slice_convert_fusion.1) | copy-start | bytes 52
  37.9 65.3 %copy-start.1 = (f32[6,1,4,64,128]{4,3,2,1,0:T(8,128)S(1)}, f32[6,1,4,64,128]{4,3,2,1,0:T(8,128)}, u32[]{:S(2)}) copy-start(f32[6,1,4,64,128]{4,3,2,1,0:T(8,128)} %get-tuple-element.33) | copy-start | bytes 2359300
  101.5 3.3 copy-start.3
  101.5 3.4 copy-start.4
  104.8 2.5 copy-start.2
  106.5 1.4 copy-start.9
  108.5 8.1 %copy-start.5 = (s32[384,2]{0,1:T(2,128)S(1)}, s32[384,2]{0,1:T(2,128)}, u32[]{:S(2)}) copy-start(s32[384,2]{0,1:T(2,128)} %param.35) | copy-start | bytes 9220
  110.1 22.5 %all-to-all-start = ((bf16[16,384,128]{2,1,0:T(8,128)(2,1)}), bf16[16,384,128]{2,1,0:T(8,128)(2,1)S(1)}, u32[]{:S(2)}, u32[]{:S(2)}) async-start(bf16[16,384,128]{2,1,0:T(8,128)(2,1)} %bitcast.250), calls=%async_computation | async-start | bytes 3145728 | tf_op jit(solution)/shard_map/all_to_all | solution.py:60
  116.4 156.2 %all-gather.10.cloned.1.call-start = ((), (), s32[]{:S(2)}) async-start(), calls=%async_computation.4 | async-start | bytes 6684672 | tf_op jit(solution)/shard_map/all_gather | solution.py:219
  132.8 139.7 %copy-start.11 = (bf16[1,2048,64]{1,2,0:T(8,128)(2,1)S(1)}, bf16[1,2048,64]{1,2,0:T(8,128)(2,1)}, u32[]{:S(2)}) copy-start(bf16[1,2048,64]{1,2,0:T(8,128)(2,1)} %param.37) | copy-start | bytes 786436
  203.5 73.8 %copy-start.12 = (bf16[1,2048,64]{1,2,0:T(8,128)(2,1)S(1)}, bf16[1,2048,64]{1,2,0:T(8,128)(2,1)}, u32[]{:S(2)}) copy-start(bf16[1,2048,64]{1,2,0:T(8,128)(2,1)} %param.38) | copy-start | bytes 786436
  203.5 150.2 %all-gather.12.cloned.1.call-start = ((), (), s32[]{:S(2)}) async-start(), calls=%async_computation.5 | async-start | bytes 3932160 | tf_op jit(solution)/shard_map/all_gather | solution.py:71
  272.6 4.8 %copy-start.10 = (bf16[32,48,2048]{2,1,0:T(8,128)(2,1)S(1)}, bf16[32,48,2048]{2,1,0:T(8,128)(2,1)}, u32[]{:S(2)}) copy-start(bf16[32,48,2048]{2,1,0:T(8,128)(2,1)} %all-gather.10.cloned.1.call-done) | copy-start | bytes 18874372
  302.5 69.2 %copy-start.7 = (f32[384,2]{0,1:T(2,128)S(1)}, f32[384,2]{0,1:T(2,128)}, u32[]{:S(2)}) copy-start(f32[384,2]{0,1:T(2,128)} %param.36) | copy-start | bytes 9220
  357.3 42.1 %all-to-all-start.2 = ((bf16[32,1,48,128]{3,2,1,0:T(8,128)(2,1)}), bf16[32,1,48,128]{3,2,1,0:T(8,128)(2,1)S(1)}, u32[]{:S(2)}, u32[]{:S(2)}) async-start(bf16[32,1,48,128]{3,2,1,0:T(8,128)(2,1)} %fusion.11), calls=%async_computation.2 | async-start | bytes 786432 | tf_op jit(solution)/shard_map/all_to_all | solution.py:230
Sparse Core Ops, SparseCore 0:
  40.9 60.5 all-gather.7
  203.6 68.9 all-gather.9
  302.7 50.9 all-gather.11
where the time goes:
time: 411 us; the launch traced here: 410 us
  waiting for transfers between devices  188 us (46%)
  blocking collectives  116 us (28%)
  local copies, waits for them, and re-layouts  26.9 us (7%)
  starting transfers between devices  25.8 us (6%)
  other arithmetic  22.7 us (6%)
  matrix products  15.9 us (4%)
  between operations  14.3 us (3%)
    all_gather x1, waiting for transfers between devices, per_device(): piece_cols = lax.all_gather(arrived, TP, axis=2, tiled=True)  69 us
    all_gather x1, waiting for transfers between devices, whole_of(): whole = lax.all_gather(whole, axes[number], axis=dim, tiled=True)  51.2 us
    all_to_all x1, blocking collectives, per_device(): lax.all_to_all(outgoing, SP, split_axis=0, concat_axis=0, tiled=True)  51.1 us
    all_gather x1, waiting for transfers between devices, entering_2(): lax.all_gather(part.astype(kind), axis)  31.5 us
    all_to_all x1, waiting for transfers between devices, per_device(): lax.all_to_all(summed.astype(jnp.bfloat16), SP, split_axis=0, concat_axis...  27.6 us
    all_gather x2, blocking collectives, entering_2(): lax.all_gather(part.astype(kind), axis)  26.1 us
    all_gather x1, blocking collectives, whole_of(): whole = lax.all_gather(whole, axes[number], axis=dim, tiled=True)  19.4 us
    all_to_all x1, starting transfers between devices, per_device(): lax.all_to_all(summed.astype(jnp.bfloat16), SP, split_axis=0, concat_axis...  14.4 us
  transfers between devices with their start and end apart: 6, of which 5 were waited for; matrix products, arithmetic and copies ran while one was open for 5% of the time, Pallas kernels for 0%

commit v1 on v0

v1 whole, which is shorter than its diff:
```python
import functools

import jax
import jax.numpy as jnp
from jax import lax
from jax.experimental import pallas as pl
from jax.experimental.pallas import tpu as pltpu
from jax.sharding import PartitionSpec as P

F32 = jnp.float32
BF16 = jnp.bfloat16
HIGH = lax.Precision.HIGHEST
EPS = 1e-06
NSP = 32
NZ = 16
NTP = 16
CAP = 48
T = 384
D = 2048
INNER = 256
STATE = 128
HEADS = 4
HD = 64
SLOTS = NSP * CAP
COLS = D // NTP
FF = 1024


def dot(a, b, dims=((1,), (0,)), precision=None):
    return lax.dot_general(a, b, (dims, ((), ())), precision=precision, preferred_element_type=F32)


def iota(shape, dim):
    return lax.broadcasted_iota(jnp.int32, shape, dim)


def silu(v):
    return v / (1.0 + jnp.exp(-v))


def kernel(
    inner, gate, wr, rd, dtx, dtt, at, taps, prm, ow, stream, fgain, ids, idst, ew, wgu, wd,
    out,
    padf, halo_x, halo_w, halo_r, lam, rlam, spc, rs, es, re, mixed, pbuf, rp, kept, ssq, rss, scol,
    pm, q0, q1, sent, rx, xb, gu, dn, hid, ob, r3, r4,
    hs, hr, ls, lr, as_, ar, bs, br, ps, pr, ss, sr, ds_, dr, fs, fr, ts, tr, us, ur, gs, gr, loc,
):
    sp = lax.axis_index("sp")
    tp = lax.axis_index("tp")
    y = tp // 4
    x = lax.rem(tp, 4)
    z = sp // 2

    def rc(src, dst, send, recv, sp_to, tp_to):
        return pltpu.make_async_remote_copy(
            src_ref=src, dst_ref=dst, send_sem=send, recv_sem=recv,
            device_id={"sp": sp_to, "tp": tp_to}, device_id_type=pl.DeviceIdType.MESH,
        )

    def tp_of(y_, x_):
        return lax.rem(y_ + 4, 4) * 4 + lax.rem(x_ + 4, 4)

    def lanes(start, size):
        return pl.ds(pl.multiple_of(start, 128), size)

    barrier = pltpu.get_barrier_semaphore()

    def greet_sp(q, carry):
        pl.semaphore_signal(
            barrier, inc=1, device_id={"sp": lax.rem(sp + q, NSP), "tp": tp},
            device_id_type=pl.DeviceIdType.MESH,
        )
        return carry

    def greet_tp(q, carry):
        pl.semaphore_signal(
            barrier, inc=1, device_id={"sp": sp, "tp": lax.rem(tp + q, NTP)},
            device_id_type=pl.DeviceIdType.MESH,
        )
        return carry

    lax.fori_loop(1, NSP, greet_sp, 0)
    lax.fori_loop(1, NTP, greet_tp, 0)

    own = lanes(tp * COLS, COLS)
    local = [
        pltpu.make_async_copy(wgu, gu.at[:, own], loc.at[0]),
        pltpu.make_async_copy(wd, dn.at[:, own], loc.at[1]),
        pltpu.make_async_copy(stream.at[:, own], scol, loc.at[2]),
    ]
    for copy in local:
        copy.start()

    lower = iota((T, T), 0) > iota((T, T), 1)
    upper = iota((T, T), 0) < iota((T, T), 1)
    e0, e1 = ids[:, 0:1], ids[:, 1:2]
    lane_e = iota((T, 128), 1)
    oh0, oh1 = lane_e == e0, lane_e == e1
    both = jnp.where(oh0 | oh1, 1.0, 0.0).astype(BF16)
    count = dot(jnp.where(lower, 1.0, 0.0).astype(BF16), both)
    t0 = e0 * CAP + jnp.sum(jnp.where(oh0, count, 0.0), axis=1, keepdims=True).astype(jnp.int32)
    t1 = e1 * CAP + jnp.sum(jnp.where(oh1, count, 0.0), axis=1, keepdims=True).astype(jnp.int32)
    for c in range(0, SLOTS, 256):
        lane = iota((T, 256), 1) + c
        q0[:, c : c + 256] = jnp.where(lane == t0, 1.0, 0.0).astype(BF16)
        q1[:, c : c + 256] = jnp.where(lane == t1, 1.0, 0.0).astype(BF16)
    e0t, e1t = idst[0:1, :], idst[1:2, :]
    sub_e = iota((NSP, T), 0)
    oh0t, oh1t = sub_e == e0t, sub_e == e1t
    botht = jnp.where(oh0t | oh1t, 1.0, 0.0).astype(BF16)
    countt = dot(botht, jnp.where(upper, 1.0, 0.0).astype(BF16))
    t0t = e0t * CAP + jnp.sum(jnp.where(oh0t, countt, 0.0), axis=0, keepdims=True).astype(jnp.int32)
    t1t = e1t * CAP + jnp.sum(jnp.where(oh1t, countt, 0.0), axis=0, keepdims=True).astype(jnp.int32)
    for c in range(0, SLOTS, 256):
        row = iota((256, T), 0) + c
        pm[c : c + 256, :] = jnp.where((row == t0t) | (row == t1t), 1.0, 0.0).astype(BF16)

    ax = dtx[...] * prm[0:1, :]
    cumx = dot(jnp.where(upper, 0.0, 1.0), ax, precision=HIGH)
    cumt = dot(at[...], jnp.where(lower, 0.0, 1.0), precision=HIGH)
    total = cumx[T - 1 : T, :]
    lam[0:1, :] = total[:, :128]
    lam[1:2, :] = total[:, 128:]

    pl.semaphore_wait(barrier, NSP - 1 + NTP - 1)

    halos = [
        rc(ref.at[T - 16 : T], dst, hs.at[n], hr.at[n], lax.rem(sp + 1, NSP), tp)
        for n, (ref, dst) in enumerate(((inner, halo_x), (wr, halo_w), (rd, halo_r)))
    ]

    @pl.when(sp < NSP - 1)
    def _():
        for copy in halos:
            copy.start()

    def sp_order(i):
        step = (i + 1) // 2
        odd = lax.rem(i, 2)
        return lax.rem(sp + 16 + step * (2 * odd - 1), NSP)

    def sp_start(src_of, dst, send, recv):
        def body(i, carry):
            e = sp_order(i)
            rc(src_of(e), dst.at[sp], send.at[e], recv.at[sp], e, tp).start()
            return carry

        lax.fori_loop(0, NSP - 1, body, 0)

    def sp_wait(src_of, dst, send, recv):
        def body(i, carry):
            e = lax.rem(sp + 1 + i, NSP)
            copy = rc(src_of(e), dst.at[e], send.at[e], recv.at[e], e, tp)
            copy.wait_send()
            copy.wait_recv()
            return carry

        lax.fori_loop(0, NSP - 1, body, 0)

    sp_start(lambda e: lam, rlam, ls, lr)

    HALF = D // 2
    HALFD = FF // 2
    parts = {
        ("gu", 0): (gu, 0, HALF),
        ("gu", 1): (gu, HALF, HALF),
        ("dn", 0): (dn, 0, HALFD),
        ("dn", 1): (dn, HALFD, HALFD),
    }
    names = list(parts)

    def neighbour(axis, step):
        return tp_of(y, x + step) if axis == 0 else tp_of(y + step, x)

    def ring_first(name, start):
        buf, r, n = parts[name]
        copies = []
        for side, step in ((0, 1), (1, -1)):
            to = neighbour(name[1], step)
            ref = buf.at[r : r + n, own]
            k = names.index(name) * 16 + side
            copies.append(rc(ref, ref, gs.at[k], gr.at[k], sp, to))
        return copies

    def ring_second(name):
        buf, r, n = parts[name]
        copies = []
        for side, step in ((0, 1), (1, -1)):
            to = neighbour(name[1], step)
            origin = neighbour(name[1], -step)
            rr = r + side * (n // 2)
            ref = buf.at[rr : rr + n // 2, lanes(origin * COLS, COLS)]
            k = names.index(name) * 16 + 2 + side
            copies.append(rc(ref, ref, gs.at[k], gr.at[k], sp, to))
        return copies

    def line_slices(name, at_y, at_x):
        if name[1] == 0:
            return [lanes(lax.rem(at_y + 4, 4) * 512, 512)]
        return [lanes(tp_of(jnp.int32(k), at_x) * COLS, COLS) for k in range(4)]

    def ring_third(name):
        buf, r, n = parts[name]
        copies = []
        for side, step in ((0, 1), (1, -1)):
            to = neighbour(1 - name[1], step)
            for j, sl in enumerate(line_slices(name, y, x)):
                ref = buf.at[r : r + n, sl]
                k = names.index(name) * 16 + 4 + side * 2
                k = ("third", name, side, j)
                copies.append(rc(ref, ref, gs.at[sem_of(k)], gr.at[sem_of(k)], sp, to))
        return copies

    def ring_fourth(name):
        buf, r, n = parts[name]
        copies = []
        for side, step in ((0, 1), (1, -1)):
            to = neighbour(1 - name[1], step)
            rr = r + side * (n // 2)
            oy, ox = (y - step, x) if name[1] == 0 else (y, x - step)
            for j, sl in enumerate(line_slices(name, oy, ox)):
                ref = buf.at[rr : rr + n // 2, sl]
                k = ("fourth", name, side, j)
                copies.append(rc(ref, ref, gs.at[sem_of(k)], gr.at[sem_of(k)], sp, to))
        return copies

    table = {}

    def sem_of(key):
        if key not in table:
            table[key] = 64 + len(table)
        return table[key]

    def start(copies):
        for copy in copies:
            copy.start()

    def recv(copies):
        for copy in copies:
            copy.wait_recv()

    def send_done(copies):
        for copy in copies:
            copy.wait_send()

    for copy in local:
        copy.wait()
    first = [c for name in names for c in ring_first(name, True)]
    start(first)

    padf[8:, :] = jnp.concatenate([inner[...], wr[...], rd[...]], axis=1).astype(F32)

    @pl.when(sp > 0)
    def _():
        for copy in halos:
            copy.wait_recv()
        tail = jnp.concatenate([halo_x[...], halo_w[...], halo_r[...]], axis=1).astype(F32)
        padf[0:8, :] = tail[8:, :]

    @pl.when(sp == 0)
    def _():
        padf[0:8, :] = jnp.zeros((8, INNER + 2 * STATE), F32)

    conv = taps[0:1, :] * padf[5 : 5 + T, :]
    for k in range(1, 4):
        conv = conv + taps[k : k + 1, :] * padf[5 + k : 5 + k + T, :]
    conv = silu(conv)
    xs = conv[:, :INNER]
    bwb = conv[:, INNER : INNER + STATE].astype(BF16)
    crb = conv[:, INNER + STATE :].astype(BF16)

    recv(first)
    second = [c for name in names for c in ring_second(name)]
    start(second)

    weighted = (xs * (jnp.exp(total - cumx) * dtx[...])).astype(BF16)
    closing = dot(bwb, weighted, ((0,), (0,))).astype(BF16)
    spc[0:16] = closing[:, :128].reshape(16, 8, 128)
    spc[16:32] = closing[:, 128:].reshape(16, 8, 128)
    sp_start(lambda e: spc.at[e], rs, as_, ar)
    rs[pl.ds(sp, 1)] = spc[pl.ds(sp, 1)]
    rlam[pl.ds(sp, 1)] = lam[...].reshape(1, 2, 128)

    head_of = iota((1, INNER), 1) >> 6
    xsb = xs.astype(BF16)
    rows = 128
    insides = []
    for c in range(0, T, rows):
        n = c + rows
        g = dot(crb[c:n], bwb[:n], ((1,), (1,)))
        causal = iota((rows, n), 0) + c >= iota((rows, n), 1)
        acc = jnp.zeros((rows, INNER), F32)
        for h in range(HEADS):
            diff = cumx[c:n, h * HD : h * HD + 1] - cumt[h : h + 1, :n]
            w = jnp.where(causal, jnp.exp(jnp.minimum(diff, 0.0)), 0.0) * g * dtt[h : h + 1, :n]
            xh = jnp.where(head_of == h, xsb[:n], jnp.zeros((), BF16))
            acc = acc + dot(w.astype(BF16), xh)
        insides.append(acc)
    inside = jnp.concatenate(insides, axis=0)

    recv(second)
    third_gu = [c for name in names[:2] for c in ring_third(name)]
    start(third_gu)

    sp_wait(lambda e: lam, rlam, ls, lr)
    sp_wait(lambda e: spc.at[e], rs, as_, ar)
    half = sp // 16

    def scan(p, carry):
        es[pl.ds(p, 1)] = carry.astype(BF16).reshape(1, 8, 128)
        decay = jnp.exp(rlam[p, pl.ds(half, 1), :])
        return carry * decay + rs[p].astype(F32)

    lax.fori_loop(0, NSP, scan, jnp.zeros((8, 128), F32))
    sp_start(lambda e: es.at[e], re, bs, br)
    re[pl.ds(sp, 1)] = es[pl.ds(sp, 1)]
    gact = silu(gate[...].astype(F32))
    grow = jnp.exp(cumx)
    sp_wait(lambda e: es.at[e], re, bs, br)
    entering = jnp.concatenate(
        [re[0:16].astype(F32).reshape(128, 128), re[16:32].astype(F32).reshape(128, 128)], axis=1
    ).astype(BF16)
    gated = (inside + dot(crb, entering) * grow) * gact
    same = jnp.where((iota((INNER, INNER), 0) >> 6) == (iota((INNER, INNER), 1) >> 6), 1.0, 0.0)
    square = dot(gated * gated, same, precision=HIGH) * (1.0 / HD)
    mixed[...] = (gated * lax.rsqrt(square + EPS) * prm[1:2, :]).astype(BF16)

    for i in range(0, NTP, 2):
        term = dot(mixed[...], ow[:, i * COLS : (i + 2) * COLS]).astype(BF16)
        pbuf[i] = term[:, :COLS]
        pbuf[i + 1] = term[:, COLS:]

    def tp_start(src_of, dst_of, send, recv_, first_=1):
        def body(i, carry):
            j = lax.rem(tp + i, NTP)
            rc(src_of(j), dst_of(tp), send.at[j], recv_.at[tp], sp, j).start()
            return carry

        lax.fori_loop(1, NTP, body, 0)

    def tp_wait(src_of, dst_of, send, recv_):
        def body(i, carry):
            j = lax.rem(tp + i, NTP)
            copy = rc(src_of(j), dst_of(j), send.at[j], recv_.at[j], sp, j)
            copy.wait_send()
            copy.wait_recv()
            return carry

        lax.fori_loop(1, NTP, body, 0)

    tp_start(lambda j: pbuf.at[j], lambda j: rp.at[j], ps, pr)
    rp[pl.ds(tp, 1)] = pbuf[pl.ds(tp, 1)]
    tp_wait(lambda j: pbuf.at[j], lambda j: rp.at[j], ps, pr)
    middle = rp[0].astype(F32)
    for i in range(1, NTP):
        middle = middle + rp[i].astype(F32)
    middle = scol[...].astype(F32) + middle
    kept[...] = middle

    ssq[...] = dot(jnp.ones((8, COLS), F32), middle * middle, ((1,), (1,)), HIGH)
    tp_start(lambda j: ssq, lambda j: rss.at[j], ss, sr)
    rss[pl.ds(tp, 1)] = ssq[...].reshape(1, 8, T)
    recv(third_gu)
    fourth_gu = [c for name in names[:2] for c in ring_fourth(name)]
    third_dn = [c for name in names[2:] for c in ring_third(name)]
    tp_wait(lambda j: ssq, lambda j: rss.at[j], ss, sr)
    start(fourth_gu)
    start(third_dn)
    sums = rss[0]
    for i in range(1, NTP):
        sums = sums + rss[i]
    scale = jnp.transpose(lax.rsqrt(sums * (1.0 / D) + EPS))[:, 0:1]
    normed = (middle * scale * fgain[:, own]).astype(BF16)
    for e in range(0, NSP, 4):
        picked = dot(pm[e * CAP : (e + 4) * CAP, :], normed).astype(BF16)
        sent[e : e + 4] = picked.reshape(4, CAP, COLS)

    sp_start(lambda e: sent.at[e], rx, ds_, dr)
    rx[pl.ds(sp, 1)] = sent[pl.ds(sp, 1)]

    def chip_order(i):
        step = (i + 1) // 2
        odd = lax.rem(i, 2)
        return lax.rem(z + step * (2 * odd - 1) + NZ, NZ)

    def forward(i, carry):
        c = chip_order(i)
        for k in range(2):
            s = 2 * c + k

            @pl.when(s != sp)
            def _():
                copy = rc(sent.at[s], rx.at[s], ds_.at[s], dr.at[s], s, tp)
                copy.wait_send()
                copy.wait_recv()

        src = rx.at[pl.ds(2 * c, 2)]

        @pl.when(c != tp)
        def _():
            rc(src, xb.at[:, :, own], fs.at[c], fr.at[tp], sp, c).start()

        @pl.when(c == tp)
        def _():
            xb[:, :, own] = rx[pl.ds(2 * c, 2)]

        return carry

    lax.fori_loop(0, NZ, forward, 0)
    recv(third_dn)
    fourth_dn = [c for name in names[2:] for c in ring_fourth(name)]
    start(fourth_dn)
    tp_wait(
        lambda j: rx.at[pl.ds(2 * j, 2)],
        lambda j: xb.at[:, :, lanes(j * COLS, COLS)],
        fs, fr,
    )
    recv(fourth_gu)

    xrow = xb[...].reshape(2 * CAP, D)
    low = iota((1, 128), 1) < 64

    def expert_in(i, carry):
        g = dot(xrow, gu[:, lanes(i * 256, 256)])
        a, b = g[:, :128], g[:, 128:]
        even = silu(a) * pltpu.roll(a, 64, 1)
        odd = silu(b) * pltpu.roll(b, 64, 1)
        hid[:, lanes(i * 128, 128)] = jnp.where(low, even, odd).astype(BF16)
        return carry

    lax.fori_loop(0, NTP // 2, expert_in, 0)
    recv(fourth_dn)
    hrow = hid[...]

    def expert_out(i, carry):
        o = dot(hrow, dn[:, lanes(i * 256, 256)]).astype(BF16)
        ob[:, :, lanes(i * 256, 256)] = o.reshape(2, CAP, 256)
        return carry

    lax.fori_loop(0, D // 256, expert_out, 0)

    tp_start(lambda j: ob.at[:, :, lanes(j * COLS, COLS)], lambda j: r3.at[j], ts, tr)
    r3[pl.ds(tp, 1)] = ob[:, :, own].reshape(1, 2, CAP, COLS)

    def give_back(i, carry):
        c = chip_order(NZ - 1 - i)

        @pl.when(c != tp)
        def _():
            copy = rc(ob.at[:, :, lanes(c * COLS, COLS)], r3.at[c], ts.at[c], tr.at[c], sp, c)
            copy.wait_send()
            copy.wait_recv()

        for k in range(2):
            s = 2 * c + k

            @pl.when(s != sp)
            def _():
                rc(r3.at[c, k], r4.at[sp], us.at[s], ur.at[sp], s, tp).start()

            @pl.when(s == sp)
            def _():
                r4[pl.ds(sp, 1)] = r3[c, pl.ds(k, 1)]

        return carry

    lax.fori_loop(0, NZ, give_back, 0)
    sp_wait(lambda e: r3.at[e // 2, lax.rem(e, 2)], r4, us, ur)

    results = r4[...].reshape(SLOTS, COLS)
    moe = dot(q0[...], results) * ew[:, 0:1] + dot(q1[...], results) * ew[:, 1:2]
    out[...] = (kept[...] + moe).astype(BF16)

    @pl.when(sp < NSP - 1)
    def _():
        for copy in halos:
            copy.wait_send()

    for copies in (first, second, third_gu, third_dn, fourth_gu, fourth_dn):
        send_done(copies)


def per_device(
    stream, inner_act, gate_act, state_write, state_read, step_raw, conv_inner, conv_write,
    conv_read, step_bias, decay_log, inner_gain, out_weight, ffn_gain, expert_ids,
    expert_weights, expert_gate, expert_up, expert_down,
):
    dt = jax.nn.softplus(step_raw.astype(F32) + step_bias[None, :])
    rate = -jnp.exp(decay_log)
    dtx = jnp.repeat(dt, HD, axis=1)
    dtt = jnp.zeros((8, T), F32).at[:HEADS].set(dt.T)
    at = jnp.zeros((8, T), F32).at[:HEADS].set((dt * rate[None, :]).T)
    taps = jnp.concatenate(
        [conv_inner, conv_write.reshape(4, STATE), conv_read.reshape(4, STATE)], axis=1
    ).astype(F32)
    prm = jnp.stack([jnp.repeat(rate, HD), inner_gain])
    idst = jnp.zeros((8, T), jnp.int32).at[:2].set(expert_ids.T)
    gate_w, up_w = expert_gate[0], expert_up[0]
    odd = lax.rem(lax.axis_index("tp"), 2) == 1
    wgu = jnp.concatenate([jnp.where(odd, up_w, gate_w), jnp.where(odd, gate_w, up_w)], axis=1)
    vmem = pl.BlockSpec(memory_space=pltpu.VMEM)
    hbm = pl.BlockSpec(memory_space=pl.ANY)
    dma = pltpu.SemaphoreType.DMA
    return pl.pallas_call(
        kernel,
        name="layer",
        out_shape=jax.ShapeDtypeStruct((T, COLS), BF16),
        in_specs=[vmem] * 10 + [hbm] + [vmem] * 4 + [hbm] * 2,
        out_specs=vmem,
        scratch_shapes=[
            pltpu.VMEM((T + 8, INNER + 2 * STATE), F32),
            pltpu.VMEM((16, INNER), BF16),
            pltpu.VMEM((16, STATE), BF16),
            pltpu.VMEM((16, STATE), BF16),
            pltpu.VMEM((2, 128), F32),
            pltpu.VMEM((NSP, 2, 128), F32),
            pltpu.VMEM((NSP, 8, 128), BF16),
            pltpu.VMEM((NSP, 8, 128), BF16),
            pltpu.VMEM((NSP, 8, 128), BF16),
            pltpu.VMEM((NSP, 8, 128), BF16),
            pltpu.VMEM((T, INNER), BF16),
            pltpu.VMEM((NTP, T, COLS), BF16),
            pltpu.VMEM((NTP, T, COLS), BF16),
            pltpu.VMEM((T, COLS), F32),
            pltpu.VMEM((8, T), F32),
            pltpu.VMEM((NTP, 8, T), F32),
            pltpu.VMEM((T, COLS), BF16),
            pltpu.VMEM((SLOTS, T), BF16),
            pltpu.VMEM((T, SLOTS), BF16),
            pltpu.VMEM((T, SLOTS), BF16),
            pltpu.VMEM((NSP, CAP, COLS), BF16),
            pltpu.VMEM((NSP, CAP, COLS), BF16),
            pltpu.VMEM((2, CAP, D), BF16),
            pltpu.VMEM((D, D), BF16),
            pltpu.VMEM((FF, D), BF16),
            pltpu.VMEM((2 * CAP, FF), BF16),
            pltpu.VMEM((2, CAP, D), BF16),
            pltpu.VMEM((NTP, 2, CAP, COLS), BF16),
            pltpu.VMEM((NSP, CAP, COLS), BF16),
            dma((3,)), dma((3,)),
            dma((NSP,)), dma((NSP,)),
            dma((NSP,)), dma((NSP,)),
            dma((NSP,)), dma((NSP,)),
            dma((NTP,)), dma((NTP,)),
            dma((NTP,)), dma((NTP,)),
            dma((NSP,)), dma((NSP,)),
            dma((NTP,)), dma((NTP,)),
            dma((NTP,)), dma((NTP,)),
            dma((NSP,)), dma((NSP,)),
            dma((112,)), dma((112,)),
            dma((3,)),
        ],
        compiler_params=pltpu.CompilerParams(
            collective_id=0, has_side_effects=True, vmem_limit_bytes=60 * 1024 * 1024
        ),
    )(
        inner_act, gate_act, state_write.reshape(T, STATE), state_read.reshape(T, STATE),
        dtx, dtt, at, taps, prm, out_weight, stream, ffn_gain.reshape(1, D), expert_ids, idst,
        expert_weights, wgu, expert_down[0],
    )


def solution(mesh):
    return jax.shard_map(
        per_device,
        mesh=mesh,
        in_specs=(
            P("sp", None), P("sp", "tp"), P("sp", "tp"), P("sp", "tp", None), P("sp", "tp", None),
            P("sp", "tp"), P(None, "tp"), P(None, "tp", None), P(None, "tp", None), P("tp"),
            P("tp"), P("tp"), P("tp", None), P(), P("sp", None), P("sp", None),
            P("sp", None, "tp"), P("sp", None, "tp"), P("sp", None, "tp"),
        ),
        out_specs=P("sp", "tp"),
        check_vma=False,
    )
```

time: 411 us -> 160 us (0.39)
  waiting for transfers between devices: 188 us -> 0 us
  Pallas kernels: 0 us -> 148 us
  blocking collectives: 116 us -> 0 us
  starting transfers between devices: 25.8 us -> 0 us
  other arithmetic: 22.7 us -> 2.44 us
  local copies, waits for them, and re-layouts: 26.9 us -> 8.6 us
  matrix products: 15.9 us -> 0 us
  between operations: 14.3 us -> 0.14 us
    all_gather x3 -> x0, waiting for transfers between devices: 152 us -> none  [the longest x1 69 us: per_device(): piece_cols = lax.all_gather(arrived, TP, axis=2, tiled=True)]
    pallas_call x0 -> x1, Pallas kernels: none -> 148 us  [per_device(): pl.pallas_call(kernel, name='layer', out_shape=jax.ShapeDtypeStruct((T, C...]
    all_to_all x1 -> x0, blocking collectives: 51.1 us -> none  [per_device(): lax.all_to_all(outgoing, SP, split_axis=0, concat_axis=0, tiled=True)]
    all_gather x3 -> x0, blocking collectives: 45.6 us -> none  [the longest x2 26.1 us: entering_2(): lax.all_gather(part.astype(kind), axis)]
    all_to_all x2 -> x0, waiting for transfers between devices: 36.3 us -> none  [the longest x1 27.6 us: per_device(): lax.all_to_all(summed.astype(jnp.bfloat16), SP, split_axis=0, concat_axis...]
    all_to_all x2 -> x0, starting transfers between devices: 20.7 us -> none  [the longest x1 14.4 us: per_device(): lax.all_to_all(summed.astype(jnp.bfloat16), SP, split_axis=0, concat_axis...]
    dot_general x8 -> x0, matrix products: 15.9 us -> none  [the longest x1 4.74 us: per_device(): jnp.einsum('secd,edf->secf', grouped, expert_gate, preferred_element_type...]
    psum x2 -> x0, blocking collectives: 14.1 us -> none  [one_axis_at_a_time(): return functools.reduce(lax.psum, axes, value)]
  transfers between devices with their start and end apart: 6 -> 0, of which waited for: 5 -> 0; matrix products, arithmetic and copies ran while one was open for 5% -> 0% of each run, Pallas kernels for 0% -> 0%
where the time goes in v1:
time: 160 us; the launch traced here: 159 us
  Pallas kernels  148 us (92%)
  local copies, waits for them, and re-layouts  8.6 us (5%)
  other arithmetic  2.44 us (2%)
    pallas_call x1, Pallas kernels, per_device(): pl.pallas_call(kernel, name='layer', out_shape=jax.ShapeDtypeStruct((T, C...  148 us
    unnamed x23, local copies, waits for them, and re-layouts  5.71 us

profile of v1, /device:TPU:1, one launch (start us, length us, event | category | flops | bytes accessed | tf_op | source)
XLA Modules:
  0.0 159.3 jit_solution(2315794692590299835)
XLA Ops:
  0.0 1.2 copy.27
  1.2 1.2 copy.28
  2.5 0.0 copy-start.8
  2.5 0.0 copy-start.1
  2.5 0.0 copy-start.7
  2.5 0.1 select_bitcast_fusion.1
  2.6 0.0 copy-start.6
  2.6 0.0 copy-start
  2.6 0.0 copy-start.2
  2.6 0.0 copy-start.3
  2.6 0.0 copy-start.4
  2.6 0.0 copy-start.5
  2.7 1.1 pad_maximum_fusion.wgu
  3.7 0.0 copy-done.8
  3.7 0.0 copy-done.1
  3.8 0.0 copy-done.7
  3.8 0.1 multiply_bitcast_fusion
  3.9 0.9 copy.31.dtx
  4.8 0.6 scatter.10.dtt
  5.4 0.6 scatter.11.at
  6.0 0.1 broadcast_in_dim.10
  6.1 0.1 stack_reshape.3
  6.2 0.0 copy-done.6
  6.2 0.6 pad_maximum_fusion.1.prm
  6.8 0.8 copy.32.ids
  7.6 0.0 copy-done.2
  7.6 0.8 copy.33.ew
  8.4 0.6 scatter.14.idst
  9.0 0.0 copy-done.3
  9.0 0.6 maximum_convert_fusion.taps
  9.6 148.1 %layer.1 = bf16[384,128]{1,0:T(8,128)(2,1)} custom-call(bf16[384,256]{1,0:T(8,128)(2,1)} %inner.1, bf16[384,256]{1,0:T(8,128)(2,1)} %gate.1, bf16[384,128]{1,0:T(8,128)(2,1)} %bitcast.18, bf16[384,128]{1,0:T(8,128)(2,1)} %bitcast.19, f32[384,256]{1,0:T(8,128)} %copy.31.dtx, f32[8,384]{1,0:T(8,128)} %scatter.10.dtt, f32[8,384]{1,0:T(8,128)} %scatter.11.at, ...), custom_call_target="tpu_custom_call" | custom-call | tf_op jit(solution)/shard_map/layer/pallas_call | solution.py:504
  157.8 1.5 copy.35
  (5 shorter events, 0.0 us)
Async XLA Ops:
  2.5 1.3 copy-start.8
  2.5 1.3 copy-start.1
  2.5 1.3 copy-start.7
  2.6 3.6 %copy-start.6 = (f32[256]{0:T(256)S(1)}, f32[256]{0:T(256)}, u32[]{:S(2)}) copy-start(f32[256]{0:T(256)} %param.36) | copy-start | bytes 3076
  2.6 4.2 %copy-start = (s32[384,2]{0,1:T(2,128)S(1)}, s32[384,2]{0,1:T(2,128)}, u32[]{:S(2)}) copy-start(s32[384,2]{0,1:T(2,128)} %param.39) | copy-start | bytes 9220
  2.6 5.0 %copy-start.2 = (f32[384,2]{0,1:T(2,128)S(1)}, f32[384,2]{0,1:T(2,128)}, u32[]{:S(2)}) copy-start(f32[384,2]{0,1:T(2,128)} %param.40) | copy-start | bytes 9220
  2.6 6.4 %copy-start.3 = (bf16[4,256]{1,0:T(4,128)(2,1)S(1)}, bf16[4,256]{1,0:T(4,128)(2,1)}, u32[]{:S(2)}) copy-start(bf16[4,256]{1,0:T(4,128)(2,1)} %param.31) | copy-start | bytes 6148
  2.6 6.4 %copy-start.4 = (bf16[4,1,128]{2,0,1:T(4,128)(2,1)S(1)}, bf16[4,1,128]{2,0,1:T(4,128)(2,1)}, u32[]{:S(2)}) copy-start(bf16[4,1,128]{2,0,1:T(4,128)(2,1)} %param.33) | copy-start | bytes 3076
  2.6 6.4 %copy-start.5 = (bf16[4,1,128]{2,0,1:T(4,128)(2,1)S(1)}, bf16[4,1,128]{2,0,1:T(4,128)(2,1)}, u32[]{:S(2)}) copy-start(bf16[4,1,128]{2,0,1:T(4,128)(2,1)} %param.32) | copy-start | bytes 3076

commit v2 on v1

v2 whole, which is shorter than its diff:
```python
import functools

import jax
import jax.numpy as jnp
from jax import lax
from jax.experimental import pallas as pl
from jax.experimental.pallas import tpu as pltpu
from jax.sharding import PartitionSpec as P

F32 = jnp.float32
BF16 = jnp.bfloat16
HIGH = lax.Precision.HIGHEST
EPS = 1e-06
NSP = 32
NZ = 16
NTP = 16
CAP = 48
T = 384
D = 2048
INNER = 256
STATE = 128
HEADS = 4
HD = 64
SLOTS = NSP * CAP
COLS = D // NTP
FF = 1024


def dot(a, b, dims=((1,), (0,)), precision=None):
    return lax.dot_general(a, b, (dims, ((), ())), precision=precision, preferred_element_type=F32)


def iota(shape, dim):
    return lax.broadcasted_iota(jnp.int32, shape, dim)


def silu(v):
    return v / (1.0 + jnp.exp(-v))


def kernel(
    raw, bias, dlog, tap_x, tap_w, tap_r, again, fgain, ids, ew,
    inner_h, gate_h, wr_h, rd_h, ow_h, stream, wg, wu, wd,
    out,
    inner, gate, wr, rd, ow, padf, halo_x, halo_w, halo_r, lam, rlam, spc, rs, es, re, colbuf, mixed, pbuf, v1, w1b, z1, s1, v2, w2b, z2, kept, ssq, rss, scol,
    pm, q0, q1, sent, rx, xb, gu, dn, hid, ob, r3, r4,
    hs, hr, ls, lr, as_, ar, bs, br, ps, pr, ss, sr, ds_, dr, fs, fr, ts, tr, us, ur, gs, gr, loc,
):
    sp = lax.axis_index("sp")
    tp = lax.axis_index("tp")
    y = tp // 4
    x = lax.rem(tp, 4)
    z = sp // 2

    def rc(src, dst, send, recv, sp_to, tp_to):
        return pltpu.make_async_remote_copy(
            src_ref=src, dst_ref=dst, send_sem=send, recv_sem=recv,
            device_id={"sp": sp_to, "tp": tp_to}, device_id_type=pl.DeviceIdType.MESH,
        )

    def tp_of(y_, x_):
        return lax.rem(y_ + 4, 4) * 4 + lax.rem(x_ + 4, 4)

    def lanes(start, size):
        return pl.ds(pl.multiple_of(start, 128), size)

    barrier = pltpu.get_barrier_semaphore()

    def greet_sp(q, carry):
        pl.semaphore_signal(
            barrier, inc=1, device_id={"sp": lax.rem(sp + q, NSP), "tp": tp},
            device_id_type=pl.DeviceIdType.MESH,
        )
        return carry

    def greet_tp(q, carry):
        pl.semaphore_signal(
            barrier, inc=1, device_id={"sp": sp, "tp": lax.rem(tp + q, NTP)},
            device_id_type=pl.DeviceIdType.MESH,
        )
        return carry

    lax.fori_loop(1, NSP, greet_sp, 0)
    lax.fori_loop(1, NTP, greet_tp, 0)

    own = lanes(tp * COLS, COLS)
    odd = lax.rem(tp, 2)
    local = [
        pltpu.make_async_copy(wg, gu.at[y, x, pl.ds(odd * 64, 64)], loc.at[0]),
        pltpu.make_async_copy(wu, gu.at[y, x, pl.ds(64 - odd * 64, 64)], loc.at[1]),
        pltpu.make_async_copy(wd, dn.at[y, x], loc.at[2]),
        pltpu.make_async_copy(inner_h, inner, loc.at[3]),
        pltpu.make_async_copy(wr_h, wr, loc.at[4]),
        pltpu.make_async_copy(rd_h, rd, loc.at[5]),
        pltpu.make_async_copy(gate_h, gate, loc.at[6]),
        pltpu.make_async_copy(ow_h, ow, loc.at[7]),
        pltpu.make_async_copy(stream.at[:, own], scol, loc.at[8]),
    ]
    for copy in local:
        copy.start()

    rate = -jnp.exp(dlog[...])
    step = raw[...].astype(F32)
    step = jnp.concatenate([step[h : h + 1] + bias[0:1, h : h + 1] for h in range(HEADS)], axis=0)
    dtt = jnp.maximum(step, 0.0) + jnp.log1p(jnp.exp(-jnp.abs(step)))
    at = jnp.concatenate(
        [dtt[h : h + 1] * rate[0:1, h : h + 1] for h in range(HEADS)] + [jnp.zeros((4, T), F32)], axis=0
    )
    colbuf[0:4, :] = dtt
    colbuf[4:6, :] = ids[...].astype(F32)
    colbuf[6:8, :] = ew[...]
    cols = jnp.transpose(colbuf[...])
    e0, e1 = cols[:, 4:5].astype(jnp.int32), cols[:, 5:6].astype(jnp.int32)
    w0, w1 = cols[:, 6:7], cols[:, 7:8]
    head_of = iota((1, INNER), 1) >> 6

    def by_head(pick):
        v = jnp.where(head_of == 0, pick(0), pick(1))
        return jnp.where(head_of == 3, pick(3), jnp.where(head_of == 2, pick(2), v))

    dtx = by_head(lambda h: cols[:, h : h + 1])
    ratex = by_head(lambda h: rate[0:1, h : h + 1])

    lower = iota((T, T), 0) > iota((T, T), 1)
    upper = iota((T, T), 0) < iota((T, T), 1)
    ax = dtx * ratex
    cumx = dot(jnp.where(upper, 0.0, 1.0), ax, precision=HIGH)
    cumt = dot(at, jnp.where(lower, 0.0, 1.0), precision=HIGH)
    total = cumx[T - 1 : T, :]
    lam[0:1, :] = total[:, :128]
    lam[1:2, :] = total[:, 128:]

    with jax.named_scope("w_barrier"):
        pl.semaphore_wait(barrier, NSP - 1 + NTP - 1)

    for copy in local[3:6]:
        copy.wait()

    halos = [
        rc(ref.at[T - 16 : T], dst, hs.at[n], hr.at[n], lax.rem(sp + 1, NSP), tp)
        for n, (ref, dst) in enumerate(((inner, halo_x), (wr, halo_w), (rd, halo_r)))
    ]

    @pl.when(sp < NSP - 1)
    def _():
        for copy in halos:
            copy.start()

    def sp_order(i):
        step = (i + 1) // 2
        odd = lax.rem(i, 2)
        return lax.rem(sp + 16 + step * (2 * odd - 1), NSP)

    def took(ref, send=None, recv=None):
        copy = rc(ref, ref, send, recv, sp, tp) if send is not None and recv is not None else None
        if copy is None:
            sem = send if send is not None else recv
            copy = rc(ref, ref, sem, sem, sp, tp)
        if send is not None:
            copy.wait_send()
        if recv is not None:
            copy.wait_recv()

    def sp_start(src_of, dst, send, recv):
        def body(i, carry):
            e = sp_order(i)
            rc(src_of(e), dst.at[sp], send.at[0], recv.at[0], e, tp).start()
            return carry

        lax.fori_loop(0, NSP - 1, body, 0)

    def sp_wait(dst, send, recv, name):
        with jax.named_scope(name):
            took(dst.at[0 : NSP - 1], send.at[0], recv.at[0])

    sp_start(lambda e: lam, rlam, ls, lr)

    half_rows = {0: COLS // 2, 1: FF // 2}

    def neighbour(axis, step):
        return tp_of(y, x + step) if axis == 0 else tp_of(y + step, x)

    def shard(buf, j, first, rows):
        return buf.at[j // 4, lax.rem(j, 4), pl.ds(first, rows)]

    def line(buf, axis, at_y, at_x, first, rows):
        if axis == 0:
            return buf.at[lax.rem(at_y + 4, 4), :, pl.ds(first, rows)]
        return buf.at[:, lax.rem(at_x + 4, 4), pl.ds(first, rows)]

    def ring(which, axis, stage, quarter=None):
        buf, n = ((gu, dn)[which], half_rows[which])
        base = axis * n
        copies = []
        for side, step in ((0, 1), (1, -1)):
            k = which * 4 + stage if quarter is None else 8 + quarter
            part = (base + side * (n // 2), n // 2) if stage % 2 else (base, n)
            if quarter is not None:
                part = (base + quarter * (n // 4), n // 4)
            if stage < 2:
                to = neighbour(axis, step)
                ref = shard(buf, tp if stage == 0 else neighbour(axis, -step), *part)
            else:
                to = neighbour(1 - axis, step)
                back = 0 if stage == 2 else step
                oy, ox = (y - back, x) if axis == 0 else (y, x - back)
                ref = line(buf, axis, oy, ox, *part)
            copies.append(rc(ref, ref, gs.at[k], gr.at[k], sp, to))
        return copies

    def rings(which, stage, quarter=None):
        return [c for axis in (0, 1) for c in ring(which, axis, stage, quarter)]

    def ring_bytes(which, stage, quarter=None):
        buf, n = ((gu, dn)[which], half_rows[which])
        rows_ = (n // 2 if stage % 2 else n) if quarter is None else n // 4
        if stage < 2:
            return buf.at[0, :, pl.ds(0, rows_)]
        return buf.at[:, :, pl.ds(0, rows_)]

    def ring_recv(which, stage, quarter=None):
        k = which * 4 + stage if quarter is None else 8 + quarter
        took(ring_bytes(which, stage, quarter), recv=gr.at[k])

    def ring_sent(which, stage, quarter=None):
        k = which * 4 + stage if quarter is None else 8 + quarter
        took(ring_bytes(which, stage, quarter), send=gs.at[k])

    def start(copies):
        for copy in copies:
            copy.start()

    for copy in local[:3]:
        copy.wait()
    first_gu, first_dn = rings(0, 0), rings(1, 0)
    start(first_gu)
    start(first_dn)

    padf[8:, :] = jnp.concatenate([inner[...], wr[...], rd[...]], axis=1).astype(F32)

    @pl.when(sp > 0)
    def _():
        for copy in halos:
            copy.wait_recv()
        tail = jnp.concatenate([halo_x[...], halo_w[...], halo_r[...]], axis=1).astype(F32)
        padf[0:8, :] = tail[8:, :]

    @pl.when(sp == 0)
    def _():
        padf[0:8, :] = jnp.zeros((8, INNER + 2 * STATE), F32)

    taps = jnp.concatenate([tap_x[...], tap_w[...], tap_r[...]], axis=1).astype(F32)
    conv = taps[0:1, :] * padf[5 : 5 + T, :]
    for k in range(1, 4):
        conv = conv + taps[k : k + 1, :] * padf[5 + k : 5 + k + T, :]
    conv = silu(conv)
    xs = conv[:, :INNER]
    bwb = conv[:, INNER : INNER + STATE].astype(BF16)
    crb = conv[:, INNER + STATE :].astype(BF16)

    weighted = (xs * (jnp.exp(total - cumx) * dtx)).astype(BF16)
    closing = dot(bwb, weighted, ((0,), (0,))).astype(BF16)
    spc[0:16] = closing[:, :128].reshape(16, 8, 128)
    spc[16:32] = closing[:, 128:].reshape(16, 8, 128)
    sp_start(lambda e: spc.at[e], rs, as_, ar)
    rs[pl.ds(sp, 1)] = spc[pl.ds(sp, 1)]
    rlam[pl.ds(sp, 1)] = lam[...].reshape(1, 2, 128)

    xsb = xs.astype(BF16)
    rows = 128
    insides = []
    for c in range(0, T, rows):
        n = c + rows
        g = dot(crb[c:n], bwb[:n], ((1,), (1,)))
        causal = iota((rows, n), 0) + c >= iota((rows, n), 1)
        acc = jnp.zeros((rows, INNER), F32)
        for h in range(HEADS):
            diff = cumx[c:n, h * HD : h * HD + 1] - cumt[h : h + 1, :n]
            w = jnp.where(causal, jnp.exp(jnp.minimum(diff, 0.0)), 0.0) * g * dtt[h : h + 1, :n]
            xh = jnp.where(head_of == h, xsb[:n], jnp.zeros((), BF16))
            acc = acc + dot(w.astype(BF16), xh)
        insides.append(acc)
    inside = jnp.concatenate(insides, axis=0)

    with jax.named_scope("w_first_gu"):
        ring_recv(0, 0)
    start(rings(0, 1))
    with jax.named_scope("w_first_dn"):
        ring_recv(1, 0)
    start(rings(1, 1))

    lane_e = iota((T, 128), 1)
    oh0, oh1 = lane_e == e0, lane_e == e1
    both = jnp.where(oh0 | oh1, 1.0, 0.0).astype(BF16)
    count = dot(jnp.where(lower, 1.0, 0.0).astype(BF16), both)
    t0 = e0 * CAP + jnp.sum(jnp.where(oh0, count, 0.0), axis=1, keepdims=True).astype(jnp.int32)
    t1 = e1 * CAP + jnp.sum(jnp.where(oh1, count, 0.0), axis=1, keepdims=True).astype(jnp.int32)
    for c in range(0, SLOTS, 256):
        lane = iota((T, 256), 1) + c
        q0[:, c : c + 256] = jnp.where(lane == t0, 1.0, 0.0).astype(BF16)
        q1[:, c : c + 256] = jnp.where(lane == t1, 1.0, 0.0).astype(BF16)
    e0t, e1t = ids[0:1, :], ids[1:2, :]
    sub_e = iota((NSP, T), 0)
    oh0t, oh1t = sub_e == e0t, sub_e == e1t
    botht = jnp.where(oh0t | oh1t, 1.0, 0.0).astype(BF16)
    countt = dot(botht, jnp.where(upper, 1.0, 0.0).astype(BF16))
    t0t = e0t * CAP + jnp.sum(jnp.where(oh0t, countt, 0.0), axis=0, keepdims=True).astype(jnp.int32)
    t1t = e1t * CAP + jnp.sum(jnp.where(oh1t, countt, 0.0), axis=0, keepdims=True).astype(jnp.int32)
    for c in range(0, SLOTS, 256):
        row = iota((256, T), 0) + c
        pm[c : c + 256, :] = jnp.where((row == t0t) | (row == t1t), 1.0, 0.0).astype(BF16)

    with jax.named_scope("w_second_gu"):
        ring_recv(0, 1)
    start(rings(0, 2, 0))
    start(rings(0, 2, 1))
    sp_wait(rlam, ls, lr, "w_lam")
    sp_wait(rs, as_, ar, "w_state1")
    half = sp // 16

    def scan(p, carry):
        es[pl.ds(p, 1)] = carry.astype(BF16).reshape(1, 8, 128)
        decay = jnp.exp(rlam[p, pl.ds(half, 1), :])
        return carry * decay + rs[p].astype(F32)

    with jax.named_scope("scan"):
        lax.fori_loop(0, NSP, scan, jnp.zeros((8, 128), F32))
    sp_start(lambda e: es.at[e], re, bs, br)
    re[pl.ds(sp, 1)] = es[pl.ds(sp, 1)]
    for copy in local[6:]:
        copy.wait()
    gact = silu(gate[...].astype(F32))
    grow = jnp.exp(cumx)
    sp_wait(re, bs, br, "w_state2")
    entering = jnp.concatenate(
        [re[0:16].astype(F32).reshape(128, 128), re[16:32].astype(F32).reshape(128, 128)], axis=1
    ).astype(BF16)
    gated = (inside + dot(crb, entering) * grow) * gact
    same = jnp.where((iota((INNER, INNER), 0) >> 6) == (iota((INNER, INNER), 1) >> 6), 1.0, 0.0)
    square = dot(gated * gated, same, precision=HIGH) * (1.0 / HD)
    mixed[...] = (gated * lax.rsqrt(square + EPS) * again[...]).astype(BF16)

    for i in range(0, NTP, 2):
        term = dot(mixed[...], ow[:, i * COLS : (i + 2) * COLS]).astype(BF16)
        pbuf[i // 4, i % 4] = term[:, :COLS]
        pbuf[i // 4, i % 4 + 1] = term[:, COLS:]

    HALF = T // 2
    PART = T // 4

    def at4(v):
        return lax.rem(v + 4, 4)

    def place(h):
        return (x, y) if h == 0 else (y, x)

    def slab(h, pos, first, rows):
        if h == 0:
            return pbuf.at[:, at4(pos), pl.ds(h * HALF + first, rows)]
        return pbuf.at[at4(pos), :, pl.ds(h * HALF + first, rows)]

    def read(h, pos, first, rows):
        if h == 0:
            v = pbuf[:, pl.ds(at4(pos), 1), h * HALF + first : h * HALF + first + rows]
        else:
            v = pbuf[pl.ds(at4(pos), 1), :, h * HALF + first : h * HALF + first + rows]
        return v.reshape(4, rows, COLS).astype(F32)

    hops = [(h, side, step) for h in (0, 1) for side, step in ((0, 1), (1, -1))]

    def hop(kind, h, side, step, src, dst):
        axis = h if kind < 3 else 1 - h
        late = kind // 3
        k = late * 3 + (0 if kind % 3 == 0 else 1 + h)
        return rc(src, dst, ps.at[kind], pr.at[k], sp, neighbour(axis, step))

    relay1, own1, sum1, relay2, own2, sum2 = [], [], [], [], [], []
    for h, side, step in hops:
        p, _ = place(h)
        relay1.append(hop(0, h, side, step, slab(h, p + 2, side * PART, PART), v1.at[h, side]))
        part = pl.ds((1 - side) * PART, PART)
        own1.append(hop(1, h, side, step, slab(h, p + step, (1 - side) * PART, PART), w1b.at[h, side, :, part]))
        part = pl.ds(side * PART, PART)
        sum1.append(hop(2, h, side, step, z1.at[h, side], w1b.at[h, side, :, part]))
    start(relay1)
    start(own1)
    with jax.named_scope("w_relay1"):
        took(v1, recv=pr.at[0])
    for n, (h, side, step) in enumerate(hops):
        p, _ = place(h)
        z1[h, side] = (read(h, p + step, side * PART, PART) + v1[h, side].astype(F32)).astype(BF16)
        sum1[n].start()
    start(rings(0, 2, 2))
    for h in (0, 1):
        p, p2 = place(h)
        with jax.named_scope("w_sum1"):
            took(w1b.at[h], recv=pr.at[1 + h])
        sums4 = read(h, p, 0, HALF) + w1b[h, 0].astype(F32) + w1b[h, 1].astype(F32)
        s1[h] = sums4.astype(BF16)
        for side, step in ((0, 1), (1, -1)):
            first_, other = pl.ds(side * PART, PART), pl.ds((1 - side) * PART, PART)
            relay2.append(hop(3, h, side, step, s1.at[h, at4(p2 + 2), first_], v2.at[h, side]))
            own2.append(hop(4, h, side, step, s1.at[h, at4(p2 + step), other], w2b.at[h, side, other]))
            sum2.append(hop(5, h, side, step, z2.at[h, side], w2b.at[h, side, first_]))
        start(relay2[2 * h : 2 * h + 2])
        start(own2[2 * h : 2 * h + 2])
    with jax.named_scope("w_relay2"):
        took(v2, recv=pr.at[3])
    for n, (h, side, step) in enumerate(hops):
        _, p2 = place(h)
        here = s1[h, pl.ds(at4(p2 + step), 1), side * PART : (side + 1) * PART].reshape(PART, COLS)
        z2[h, side] = (here.astype(F32) + v2[h, side].astype(F32)).astype(BF16)
        sum2[n].start()
    start(rings(0, 2, 3))
    halves = []
    for h in (0, 1):
        p, p2 = place(h)
        with jax.named_scope("w_sum2"):
            took(w2b.at[h], recv=pr.at[4 + h])
        mine = pbuf[pl.ds(y, 1), pl.ds(x, 1), h * HALF : (h + 1) * HALF].reshape(HALF, COLS).astype(F32)
        for side in (0, 1):
            mine = mine + w1b[h, side, pl.ds(p2, 1)].reshape(HALF, COLS).astype(F32)
        halves.append(mine + w2b[h, 0].astype(F32) + w2b[h, 1].astype(F32))
    middle = scol[...].astype(F32) + jnp.concatenate(halves, axis=0)
    kept[...] = middle

    ssq[...] = dot(jnp.ones((8, COLS), F32), middle * middle, ((1,), (1,)), HIGH)
    def tell(i, carry):
        j = lax.rem(tp + i, NTP)
        rc(ssq, rss.at[tp], ss.at[0], sr.at[0], sp, j).start()
        return carry

    lax.fori_loop(1, NTP, tell, 0)
    rss[pl.ds(tp, 1)] = ssq[...].reshape(1, 8, T)
    with jax.named_scope("w_second_dn"):
        ring_recv(1, 1)
    start(rings(1, 2))
    with jax.named_scope("w_ssq"):
        took(rss.at[0 : NTP - 1], ss.at[0], sr.at[0])
    sums = rss[0]
    for i in range(1, NTP):
        sums = sums + rss[i]
    scale = jnp.transpose(lax.rsqrt(sums * (1.0 / D) + EPS))[:, 0:1]
    normed = (middle * scale * fgain[:, own]).astype(BF16)
    for e in range(0, NSP, 4):
        picked = dot(pm[e * CAP : (e + 4) * CAP, :], normed).astype(BF16)
        sent[e : e + 4] = picked.reshape(4, CAP, COLS)

    def dispatch(i, carry):
        e = sp_order(i)
        rc(sent.at[e], rx.at[sp], ds_.at[0], dr.at[z], e, tp).start()
        return carry

    lax.fori_loop(0, NSP - 1, dispatch, 0)
    rx[pl.ds(sp, 1)] = sent[pl.ds(sp, 1)]

    def chip_order(i):
        step = (i + 1) // 2
        odd = lax.rem(i, 2)
        return lax.rem(z + step * (2 * odd - 1) + NZ, NZ)

    def forward(i, carry):
        c = chip_order(NZ - 1 - i)
        @pl.when(c != z)
        def _():
            took(rx.at[pl.ds(2 * c, 2)], recv=dr.at[c])

        @pl.when(c == z)
        def _():
            took(rx.at[2 * c], recv=dr.at[c])

        src = rx.at[pl.ds(2 * c, 2)]

        @pl.when(c != tp)
        def _():
            rc(src, xb.at[:, :, own], fs.at[0], fr.at[0], sp, c).start()

        @pl.when(c == tp)
        def _():
            xb[:, :, own] = rx[pl.ds(2 * c, 2)]

        return carry

    with jax.named_scope("w_third_gu"):
        for q in range(4):
            ring_recv(0, 2, q)
    start(rings(0, 3))
    with jax.named_scope("forward"):
        lax.fori_loop(0, NZ, forward, 0)
    with jax.named_scope("w_third_dn"):
        ring_recv(1, 2)
    start(rings(1, 3))
    with jax.named_scope("w_fwd"):
        took(r3.at[0 : NTP - 1], fs.at[0], fr.at[0])
    with jax.named_scope("w_fourth_gu"):
        ring_recv(0, 3)

    xrow = xb[...].reshape(2 * CAP, D)
    low = iota((1, 128), 1) < 64

    def expert_in(i, carry):
        q = 2 * lax.rem(i, 2)
        w = gu[i // 2, pl.ds(q, 2)].reshape(256, D)
        g = dot(xrow, w, ((1,), (1,)))
        a, b = g[:, :128], g[:, 128:]
        even = silu(a) * pltpu.roll(a, 64, 1)
        odd = silu(b) * pltpu.roll(b, 64, 1)
        hid[:, lanes(i * 128, 128)] = jnp.where(low, even, odd).astype(BF16)
        return carry

    with jax.named_scope("expert_in"):
        lax.fori_loop(0, NTP // 2, expert_in, 0)
    with jax.named_scope("w_fourth_dn"):
        ring_recv(1, 3)
    hrow = hid[...]

    def expert_out(i, carry):
        i = lax.rem(i + tp // 2, NTP // 2)
        q = 2 * lax.rem(i, 2)
        w = jnp.concatenate([dn[i // 2, q], dn[i // 2, q + 1]], axis=1)
        o = dot(hrow, w).astype(BF16)
        ob[:, :, lanes(i * 256, 256)] = o.reshape(2, CAP, 256)
        for k in range(2):
            j = 2 * i + k

            @pl.when(j != tp)
            def _():
                rc(ob.at[:, :, lanes(j * COLS, COLS)], r3.at[tp], ts.at[0], tr.at[tp], sp, j).start()

        return carry

    with jax.named_scope("expert_out"):
        lax.fori_loop(0, D // 256, expert_out, 0)

    r3[pl.ds(tp, 1)] = ob[:, :, own].reshape(1, 2, CAP, COLS)

    def give_back(i, carry):
        c = chip_order(NZ - 1 - i)

        @pl.when(c != tp)
        def _():
            took(r3.at[c], recv=tr.at[c])

        for k in range(2):
            s = 2 * c + k

            @pl.when(s != sp)
            def _():
                rc(r3.at[c, k], r4.at[sp], us.at[0], ur.at[0], s, tp).start()

            @pl.when(s == sp)
            def _():
                r4[pl.ds(sp, 1)] = r3[c, pl.ds(k, 1)]

        return carry

    with jax.named_scope("give_back"):
        lax.fori_loop(0, NZ, give_back, 0)
    sp_wait(r4, us, ur, "w_ret")

    results = r4[...].reshape(SLOTS, COLS)
    moe = dot(q0[...], results) * w0 + dot(q1[...], results) * w1
    out[...] = kept[...] + moe

    @pl.when(sp < NSP - 1)
    def _():
        for copy in halos:
            copy.wait_send()

    with jax.named_scope("sends"):
        took(r4.at[0 : NSP - 1], send=ds_.at[0])
        took(r3.at[0 : NTP - 1], send=ts.at[0])
        for kind, ref in enumerate((v1, v1, v1, v2, v2, v2)):
            took(ref, send=ps.at[kind])
        for which in (0, 1):
            for stage in range(4):
                if which == 0 and stage == 2:
                    for q in range(4):
                        ring_sent(0, 2, q)
                else:
                    ring_sent(which, stage)


def per_device(
    stream, inner_act, gate_act, state_write, state_read, step_raw, conv_inner, conv_write,
    conv_read, step_bias, decay_log, inner_gain, out_weight, ffn_gain, expert_ids,
    expert_weights, expert_gate, expert_up, expert_down,
):
    vmem = pl.BlockSpec(memory_space=pltpu.VMEM)
    hbm = pl.BlockSpec(memory_space=pl.ANY)
    dma = pltpu.SemaphoreType.DMA
    return pl.pallas_call(
        kernel,
        name="layer",
        out_shape=jax.ShapeDtypeStruct((T, COLS), F32),
        in_specs=[vmem] * 10 + [hbm] * 9,
        out_specs=vmem,
        scratch_shapes=[
            pltpu.VMEM((T, INNER), BF16),
            pltpu.VMEM((T, INNER), BF16),
            pltpu.VMEM((T, STATE), BF16),
            pltpu.VMEM((T, STATE), BF16),
            pltpu.VMEM((INNER, D), BF16),
            pltpu.VMEM((T + 8, INNER + 2 * STATE), F32),
            pltpu.VMEM((16, INNER), BF16),
            pltpu.VMEM((16, STATE), BF16),
            pltpu.VMEM((16, STATE), BF16),
            pltpu.VMEM((2, 128), F32),
            pltpu.VMEM((NSP, 2, 128), F32),
            pltpu.VMEM((NSP, 8, 128), BF16),
            pltpu.VMEM((NSP, 8, 128), BF16),
            pltpu.VMEM((NSP, 8, 128), BF16),
            pltpu.VMEM((NSP, 8, 128), BF16),
            pltpu.VMEM((8, T), F32),
            pltpu.VMEM((T, INNER), BF16),
            pltpu.VMEM((4, 4, T, COLS), BF16),
            pltpu.VMEM((2, 2, 4, T // 4, COLS), BF16),
            pltpu.VMEM((2, 2, 4, T // 2, COLS), BF16),
            pltpu.VMEM((2, 2, 4, T // 4, COLS), BF16),
            pltpu.VMEM((2, 4, T // 2, COLS), BF16),
            pltpu.VMEM((2, 2, T // 4, COLS), BF16),
            pltpu.VMEM((2, 2, T // 2, COLS), BF16),
            pltpu.VMEM((2, 2, T // 4, COLS), BF16),
            pltpu.VMEM((T, COLS), F32),
            pltpu.VMEM((8, T), F32),
            pltpu.VMEM((NTP, 8, T), F32),
            pltpu.VMEM((T, COLS), BF16),
            pltpu.VMEM((SLOTS, T), BF16),
            pltpu.VMEM((T, SLOTS), BF16),
            pltpu.VMEM((T, SLOTS), BF16),
            pltpu.VMEM((NSP, CAP, COLS), BF16),
            pltpu.VMEM((NSP, CAP, COLS), BF16),
            pltpu.VMEM((2, CAP, D), BF16),
            pltpu.VMEM((4, 4, COLS, D), BF16),
            pltpu.VMEM((4, 4, FF, COLS), BF16),
            pltpu.VMEM((2 * CAP, FF), BF16),
            pltpu.VMEM((2, CAP, D), BF16),
            pltpu.VMEM((NTP, 2, CAP, COLS), BF16),
            pltpu.VMEM((NSP, CAP, COLS), BF16),
            dma((3,)), dma((3,)),
            dma((1,)), dma((1,)),
            dma((1,)), dma((1,)),
            dma((1,)), dma((1,)),
            dma((6,)), dma((6,)),
            dma((1,)), dma((1,)),
            dma((1,)), dma((NZ,)),
            dma((1,)), dma((1,)),
            dma((1,)), dma((NTP,)),
            dma((1,)), dma((1,)),
            dma((12,)), dma((12,)),
            dma((9,)),
        ],
        compiler_params=pltpu.CompilerParams(
            collective_id=0, has_side_effects=True, vmem_limit_bytes=60 * 1024 * 1024
        ),
    )(
        step_raw.T, step_bias.reshape(1, HEADS), decay_log.reshape(1, HEADS), conv_inner,
        conv_write.reshape(4, STATE), conv_read.reshape(4, STATE), inner_gain.reshape(1, INNER),
        ffn_gain.reshape(1, D), expert_ids.T, expert_weights.T,
        inner_act, gate_act, state_write.reshape(T, STATE), state_read.reshape(T, STATE),
        out_weight, stream, expert_gate[0].T, expert_up[0].T, expert_down[0],
    ).astype(BF16    )


def solution(mesh):
    return jax.shard_map(
        per_device,
        mesh=mesh,
        in_specs=(
            P("sp", None), P("sp", "tp"), P("sp", "tp"), P("sp", "tp", None), P("sp", "tp", None),
            P("sp", "tp"), P(None, "tp"), P(None, "tp", None), P(None, "tp", None), P("tp"),
            P("tp"), P("tp"), P("tp", None), P(), P("sp", None), P("sp", None),
            P("sp", None, "tp"), P("sp", None, "tp"), P("sp", None, "tp"),
        ),
        out_specs=P("sp", "tp"),
        check_vma=False,
    )
```

time: 160 us -> 126 us (0.79)
  Pallas kernels: 148 us -> 124 us
  local copies, waits for them, and re-layouts: 8.6 us -> 0 us
    pallas_call x1, Pallas kernels: 148 us -> 124 us  [per_device(): pl.pallas_call(kernel, name='layer', out_shape=jax.ShapeDtypeStruct((T, C...]
    unnamed x23 -> x0, local copies, waits for them, and re-layouts: 5.71 us -> none
    scatter x3 -> x0, local copies, waits for them, and re-layouts: 1.8 us -> none  [the longest x1 0.6 us: per_device(): dtt = jnp.zeros((8, T), F32).at[:HEADS].set(dt.T)]
where the time goes in v2:
time: 126 us
  Pallas kernels  124 us (98%)
  other arithmetic  1.58 us (1%)
    pallas_call x1, Pallas kernels, per_device(): pl.pallas_call(kernel, name='layer', out_shape=jax.ShapeDtypeStruct((T, C...  124 us

profile of v2, /device:TPU:1, one launch (start us, length us, event | category | flops | bytes accessed | tf_op | source)
XLA Modules:
  0.0 125.7 jit_solution(14235558115631727103)
XLA Ops:
  0.0 124.2 %layer.1 = f32[384,128]{1,0:T(8,128)} custom-call(bf16[4,384]{1,0:T(4,128)(2,1)} %bitcast.24, f32[1,4]{1,0:T(1,128)} %bitcast.30, f32[1,4]{1,0:T(1,128)} %bitcast.31, bf16[4,256]{1,0:T(4,128)(2,1)} %tap_x.1, bf16[4,128]{1,0:T(4,128)(2,1)} %bitcast.27, bf16[4,128]{1,0:T(4,128)(2,1)} %bitcast.28, f32[1,256]{1,0:T(1,128)} %bitcast.29, f32[1,2048]{1,0:T(1,128)} %bitcast.23, ...), custom_call_target="tpu_custom_call" | custom-call | tf_op jit(solution)/shard_map/layer/pallas_call | solution.py:592
  124.2 1.6 %convert_element_type.3 = bf16[384,128]{1,0:T(8,128)(2,1)} convert(f32[384,128]{1,0:T(8,128)} %layer.1) | non-fusion elementwise | flops 49152 | bytes 294912 | tf_op jit(solution)/shard_map/convert_element_type | solution.py:662

commit v3 on v2

--- a/solution.py
+++ b/solution.py
@@ -39,12 +39,12 @@
 
 
 def kernel(
-    raw, bias, dlog, tap_x, tap_w, tap_r, again, fgain, ids, ew,
+    raw_h, bias_h, dlog_h, tap_xh, tap_wh, tap_rh, again_h, fgain_h, ids_h, ew_h,
     inner_h, gate_h, wr_h, rd_h, ow_h, stream, wg, wu, wd,
     out,
-    inner, gate, wr, rd, ow, padf, halo_x, halo_w, halo_r, lam, rlam, spc, rs, es, re, colbuf, mixed, pbuf, v1, w1b, z1, s1, v2, w2b, z2, kept, ssq, rss, scol,
-    pm, q0, q1, sent, rx, xb, gu, dn, hid, ob, r3, r4,
-    hs, hr, ls, lr, as_, ar, bs, br, ps, pr, ss, sr, ds_, dr, fs, fr, ts, tr, us, ur, gs, gr, loc,
+    raw, bias, dlog, tap_x, tap_w, tap_r, again, fgain, ids, ew, inner, gate, wr, rd, ow, padf, halo_x, halo_w, halo_r, lam, rlam, spc, rs, es, re, colbuf, mixed, pbuf, v1, w1b, z1, s1, v2, w2b, z2, kept, scol,
+    pm, q0, q1, sent, rx, xb, xn, gu, dn, hid, ob, r3, r4,
+    hs, hr, ls, lr, as_, ar, bs, br, ps, pr, ds_, dr, fs, fr, ts, tr, us, ur, es_, er, gs, gr, loc,
 ):
     sp = lax.axis_index("sp")
     tp = lax.axis_index("tp")
@@ -88,7 +88,7 @@
     local = [
         pltpu.make_async_copy(wg, gu.at[y, x, pl.ds(odd * 64, 64)], loc.at[0]),
         pltpu.make_async_copy(wu, gu.at[y, x, pl.ds(64 - odd * 64, 64)], loc.at[1]),
-        pltpu.make_async_copy(wd, dn.at[y, x], loc.at[2]),
+        pltpu.make_async_copy(wd, dn.at[x], loc.at[2]),
         pltpu.make_async_copy(inner_h, inner, loc.at[3]),
         pltpu.make_async_copy(wr_h, wr, loc.at[4]),
         pltpu.make_async_copy(rd_h, rd, loc.at[5]),
@@ -96,8 +96,127 @@
         pltpu.make_async_copy(ow_h, ow, loc.at[7]),
         pltpu.make_async_copy(stream.at[:, own], scol, loc.at[8]),
     ]
-    for copy in local:
+    small = [
+        pltpu.make_async_copy(src, dst, loc.at[9 + n])
+        for n, (src, dst) in enumerate((
+            (raw_h, raw), (bias_h, bias), (dlog_h, dlog), (tap_xh, tap_x), (tap_wh, tap_w),
+            (tap_rh, tap_r), (again_h, again), (fgain_h, fgain), (ids_h, ids), (ew_h, ew),
+        ))
+    ]
+    for copy in small + local:
         copy.start()
+
+    with jax.named_scope("w_barrier"):
+        pl.semaphore_wait(barrier, NSP - 1 + NTP - 1)
+
+    def sp_order(i):
+        step = (i + 1) // 2
+        odd = lax.rem(i, 2)
+        return lax.rem(sp + 16 + step * (2 * odd - 1), NSP)
+
+    def took(ref, send=None, recv=None):
+        copy = rc(ref, ref, send, recv, sp, tp) if send is not None and recv is not None else None
+        if copy is None:
+            sem = send if send is not None else recv
+            copy = rc(ref, ref, sem, sem, sp, tp)
+        if send is not None:
+            copy.wait_send()
+        if recv is not None:
+            copy.wait_recv()
+
+    def sp_start(src_of, dst, send, recv):
+        def body(i, carry):
+            e = sp_order(i)
+            rc(src_of(e), dst.at[sp], send.at[0], recv.at[0], e, tp).start()
+            return carry
+
+        lax.fori_loop(0, NSP - 1, body, 0)
+
+    def sp_wait(dst, send, recv, name):
+        with jax.named_scope(name):
+            took(dst.at[0 : NSP - 1], send.at[0], recv.at[0])
+
+    def neighbour(axis, step):
+        return tp_of(y, x + step) if axis == 0 else tp_of(y + step, x)
+
+    QN = COLS // 2
+
+    def at4(v):
+        return lax.rem(v + 4, 4)
+
+    def ring(axis, stage, quarter=None, piece=None):
+        base = axis * QN
+        copies = []
+        for side, step in ((0, 1), (1, -1)):
+            k = stage if quarter is None else 4 + quarter
+            part = pl.ds(*((base + side * (QN // 2), QN // 2) if stage % 2 else (base, QN)))
+            if quarter is not None:
+                part = pl.ds(base + quarter * (QN // 4), QN // 4)
+            back = step if stage % 2 else 0
+            if stage < 2:
+                to = neighbour(axis, step)
+                oy, ox = (y, at4(x - back)) if axis == 0 else (at4(y - back), x)
+                ref = gu.at[oy, ox, part]
+            else:
+                to = neighbour(1 - axis, step)
+                wide = slice(None) if piece is None else pl.ds(piece * (D // 4), D // 4)
+                if axis == 0:
+                    ref = gu.at[at4(y - back), :, part, wide]
+                else:
+                    ref = gu.at[:, at4(x - back), part, wide]
+            copies.append(rc(ref, ref, gs.at[k], gr.at[k], sp, to))
+        return copies
+
+    def ring_dn(stage, piece=0):
+        copies = []
+        for side, step in ((0, 1), (1, -1)):
+            own_rows = pl.ds(piece * (FF // 2), FF // 2)
+            ref = dn.at[x, own_rows] if stage == 0 else dn.at[at4(x - step), pl.ds(side * (FF // 2), FF // 2)]
+            copies.append(rc(ref, ref, gs.at[8 + stage], gr.at[8 + stage], sp, tp_of(y, x + step)))
+        return copies
+
+    def rings(stage, quarter=None, piece=None):
+        return [c for axis in (0, 1) for c in ring(axis, stage, quarter, piece)]
+
+    def ring_bytes(stage, quarter=None):
+        rows_ = (QN // 2 if stage % 2 else QN) if quarter is None else QN // 4
+        if stage < 2:
+            return gu.at[0, :, pl.ds(0, rows_)]
+        return gu.at[:, :, pl.ds(0, rows_)]
+
+    def ring_recv(stage, quarter=None):
+        took(ring_bytes(stage, quarter), recv=gr.at[stage if quarter is None else 4 + quarter])
+
+    def ring_sent(stage, quarter=None):
+        took(ring_bytes(stage, quarter), send=gs.at[stage if quarter is None else 4 + quarter])
+
+    def dn_bytes(stage):
+        return dn.at[0:2] if stage == 0 else dn.at[0]
+
+    def start(copies):
+        for copy in copies:
+            copy.start()
+
+    for copy in local[:3]:
+        copy.wait()
+    start(rings(0))
+    start(ring_dn(0, 0))
+
+    for copy in local[3:6]:
+        copy.wait()
+
+    halos = [
+        rc(ref.at[T - 16 : T], dst, hs.at[n], hr.at[n], lax.rem(sp + 1, NSP), tp)
+        for n, (ref, dst) in enumerate(((inner, halo_x), (wr, halo_w), (rd, halo_r)))
+    ]
+
+    @pl.when(sp < NSP - 1)
+    def _():
+        for copy in halos:
+            copy.start()
+
+    for copy in small:
+        copy.wait()
 
     rate = -jnp.exp(dlog[...])
     step = raw[...].astype(F32)
@@ -130,111 +249,7 @@
     lam[0:1, :] = total[:, :128]
     lam[1:2, :] = total[:, 128:]
 
-    with jax.named_scope("w_barrier"):
-        pl.semaphore_wait(barrier, NSP - 1 + NTP - 1)
-
-    for copy in local[3:6]:
-        copy.wait()
-
-    halos = [
-        rc(ref.at[T - 16 : T], dst, hs.at[n], hr.at[n], lax.rem(sp + 1, NSP), tp)
-        for n, (ref, dst) in enumerate(((inner, halo_x), (wr, halo_w), (rd, halo_r)))
-    ]
-
-    @pl.when(sp < NSP - 1)
-    def _():
-        for copy in halos:
-            copy.start()
-
-    def sp_order(i):
-        step = (i + 1) // 2
-        odd = lax.rem(i, 2)
-        return lax.rem(sp + 16 + step * (2 * odd - 1), NSP)
-
-    def took(ref, send=None, recv=None):
-        copy = rc(ref, ref, send, recv, sp, tp) if send is not None and recv is not None else None
-        if copy is None:
-            sem = send if send is not None else recv
-            copy = rc(ref, ref, sem, sem, sp, tp)
-        if send is not None:
-            copy.wait_send()
-        if recv is not None:
-            copy.wait_recv()
-
-    def sp_start(src_of, dst, send, recv):
-        def body(i, carry):
-            e = sp_order(i)
-            rc(src_of(e), dst.at[sp], send.at[0], recv.at[0], e, tp).start()
-            return carry
-
-        lax.fori_loop(0, NSP - 1, body, 0)
-
-    def sp_wait(dst, send, recv, name):
-        with jax.named_scope(name):
-            took(dst.at[0 : NSP - 1], send.at[0], recv.at[0])
-
     sp_start(lambda e: lam, rlam, ls, lr)
-
-    half_rows = {0: COLS // 2, 1: FF // 2}
-
-    def neighbour(axis, step):
-        return tp_of(y, x + step) if axis == 0 else tp_of(y + step, x)
-
-    def shard(buf, j, first, rows):
-        return buf.at[j // 4, lax.rem(j, 4), pl.ds(first, rows)]
-
-    def line(buf, axis, at_y, at_x, first, rows):
-        if axis == 0:
-            return buf.at[lax.rem(at_y + 4, 4), :, pl.ds(first, rows)]
-        return buf.at[:, lax.rem(at_x + 4, 4), pl.ds(first, rows)]
-
-    def ring(which, axis, stage, quarter=None):
-        buf, n = ((gu, dn)[which], half_rows[which])
-        base = axis * n
-        copies = []
-        for side, step in ((0, 1), (1, -1)):
-            k = which * 4 + stage if quarter is None else 8 + quarter
-            part = (base + side * (n // 2), n // 2) if stage % 2 else (base, n)
-            if quarter is not None:
-                part = (base + quarter * (n // 4), n // 4)
-            if stage < 2:
-                to = neighbour(axis, step)
-                ref = shard(buf, tp if stage == 0 else neighbour(axis, -step), *part)
-            else:
-                to = neighbour(1 - axis, step)
-                back = 0 if stage == 2 else step
-                oy, ox = (y - back, x) if axis == 0 else (y, x - back)
-                ref = line(buf, axis, oy, ox, *part)
-            copies.append(rc(ref, ref, gs.at[k], gr.at[k], sp, to))
-        return copies
-
-    def rings(which, stage, quarter=None):
-        return [c for axis in (0, 1) for c in ring(which, axis, stage, quarter)]
-
-    def ring_bytes(which, stage, quarter=None):
-        buf, n = ((gu, dn)[which], half_rows[which])
-        rows_ = (n // 2 if stage % 2 else n) if quarter is None else n // 4
-        if stage < 2:
-            return buf.at[0, :, pl.ds(0, rows_)]
-        return buf.at[:, :, pl.ds(0, rows_)]
-
-    def ring_recv(which, stage, quarter=None):
-        k = which * 4 + stage if quarter is None else 8 + quarter
-        took(ring_bytes(which, stage, quarter), recv=gr.at[k])
-
-    def ring_sent(which, stage, quarter=None):
-        k = which * 4 + stage if quarter is None else 8 + quarter
-        took(ring_bytes(which, stage, quarter), send=gs.at[k])
-
-    def start(copies):
-        for copy in copies:
-            copy.start()
-
-    for copy in local[:3]:
-        copy.wait()
-    first_gu, first_dn = rings(0, 0), rings(1, 0)
-    start(first_gu)
-    start(first_dn)
 
     padf[8:, :] = jnp.concatenate([inner[...], wr[...], rd[...]], axis=1).astype(F32)
 
@@ -283,11 +298,9 @@
     inside = jnp.concatenate(insides, axis=0)
 
     with jax.named_scope("w_first_gu"):
-        ring_recv(0, 0)
-    start(rings(0, 1))
-    with jax.named_scope("w_first_dn"):
-        ring_recv(1, 0)
-    start(rings(1, 1))
+        ring_recv(0)
+    start(rings(1))
+    start(ring_dn(0, 1))
 
     lane_e = iota((T, 128), 1)
     oh0, oh1 = lane_e == e0, lane_e == e1
@@ -310,10 +323,6 @@
         row = iota((256, T), 0) + c
         pm[c : c + 256, :] = jnp.where((row == t0t) | (row == t1t), 1.0, 0.0).astype(BF16)
 
-    with jax.named_scope("w_second_gu"):
-        ring_recv(0, 1)
-    start(rings(0, 2, 0))
-    start(rings(0, 2, 1))
     sp_wait(rlam, ls, lr, "w_lam")
     sp_wait(rs, as_, ar, "w_state1")
     half = sp // 16
@@ -326,6 +335,10 @@
     with jax.named_scope("scan"):
         lax.fori_loop(0, NSP, scan, jnp.zeros((8, 128), F32))
     sp_start(lambda e: es.at[e], re, bs, br)
+    with jax.named_scope("w_second_gu"):
+        ring_recv(1)
+    start(rings(2, 0))
+    start(rings(2, 1, 0))
     re[pl.ds(sp, 1)] = es[pl.ds(sp, 1)]
     for copy in local[6:]:
         copy.wait()
@@ -347,9 +360,6 @@
 
     HALF = T // 2
     PART = T // 4
-
-    def at4(v):
-        return lax.rem(v + 4, 4)
 
     def place(h):
         return (x, y) if h == 0 else (y, x)
@@ -390,7 +400,7 @@
         p, _ = place(h)
         z1[h, side] = (read(h, p + step, side * PART, PART) + v1[h, side].astype(F32)).astype(BF16)
         sum1[n].start()
-    start(rings(0, 2, 2))
+    start(rings(2, 1, 1))
     for h in (0, 1):
         p, p2 = place(h)
         with jax.named_scope("w_sum1"):
@@ -404,6 +414,7 @@
             sum2.append(hop(5, h, side, step, z2.at[h, side], w2b.at[h, side, first_]))
         start(relay2[2 * h : 2 * h + 2])
         start(own2[2 * h : 2 * h + 2])
+    start(rings(2, 1, 2))
     with jax.named_scope("w_relay2"):
         took(v2, recv=pr.at[3])
     for n, (h, side, step) in enumerate(hops):
@@ -411,7 +422,11 @@
         here = s1[h, pl.ds(at4(p2 + step), 1), side * PART : (side + 1) * PART].reshape(PART, COLS)
         z2[h, side] = (here.astype(F32) + v2[h, side].astype(F32)).astype(BF16)
         sum2[n].start()
-    start(rings(0, 2, 3))
+    start(rings(2, 1, 3))
+    start(rings(2, 2))
+    start(rings(2, 3))
+    took(dn_bytes(0), recv=gr.at[8])
+    start(ring_dn(1))
     halves = []
     for h in (0, 1):
         p, p2 = place(h)
@@ -424,26 +439,9 @@
     middle = scol[...].astype(F32) + jnp.concatenate(halves, axis=0)
     kept[...] = middle
 
-    ssq[...] = dot(jnp.ones((8, COLS), F32), middle * middle, ((1,), (1,)), HIGH)
-    def tell(i, carry):
-        j = lax.rem(tp + i, NTP)
-        rc(ssq, rss.at[tp], ss.at[0], sr.at[0], sp, j).start()
-        return carry
-
-    lax.fori_loop(1, NTP, tell, 0)
-    rss[pl.ds(tp, 1)] = ssq[...].reshape(1, 8, T)
-    with jax.named_scope("w_second_dn"):
-        ring_recv(1, 1)
-    start(rings(1, 2))
-    with jax.named_scope("w_ssq"):
-        took(rss.at[0 : NTP - 1], ss.at[0], sr.at[0])
-    sums = rss[0]
-    for i in range(1, NTP):
-        sums = sums + rss[i]
-    scale = jnp.transpose(lax.rsqrt(sums * (1.0 / D) + EPS))[:, 0:1]
-    normed = (middle * scale * fgain[:, own]).astype(BF16)
+    rows16 = middle.astype(BF16)
     for e in range(0, NSP, 4):
-        picked = dot(pm[e * CAP : (e + 4) * CAP, :], normed).astype(BF16)
+        picked = dot(pm[e * CAP : (e + 4) * CAP, :], rows16).astype(BF16)
         sent[e : e + 4] = picked.reshape(4, CAP, COLS)
 
     def dispatch(i, carry):
@@ -483,64 +481,42 @@
 
     with jax.named_scope("w_third_gu"):
         for q in range(4):
-            ring_recv(0, 2, q)
-    start(rings(0, 3))
+            ring_recv(2, q)
+    start(rings(3))
     with jax.named_scope("forward"):
         lax.fori_loop(0, NZ, forward, 0)
-    with jax.named_scope("w_third_dn"):
-        ring_recv(1, 2)
-    start(rings(1, 3))
     with jax.named_scope("w_fwd"):
-        took(r3.at[0 : NTP - 1], fs.at[0], fr.at[0])
+        took(r3.at[0 : NTP - 1], recv=fr.at[0])
+    xf = xb[...].reshape(2 * CAP, D).astype(F32)
+    mean = jnp.sum(xf * xf, axis=1, keepdims=True) * (1.0 / D)
+    xn[...] = (xf * lax.rsqrt(mean + EPS) * fgain[...]).astype(BF16)
     with jax.named_scope("w_fourth_gu"):
-        ring_recv(0, 3)
-
-    xrow = xb[...].reshape(2 * CAP, D)
+        ring_recv(3)
+
     low = iota((1, 128), 1) < 64
 
     def expert_in(i, carry):
         q = 2 * lax.rem(i, 2)
         w = gu[i // 2, pl.ds(q, 2)].reshape(256, D)
-        g = dot(xrow, w, ((1,), (1,)))
+        g = dot(xn[...], w, ((1,), (1,)))
         a, b = g[:, :128], g[:, 128:]
         even = silu(a) * pltpu.roll(a, 64, 1)
         odd = silu(b) * pltpu.roll(b, 64, 1)
-        hid[:, lanes(i * 128, 128)] = jnp.where(low, even, odd).astype(BF16)
+        units = lanes(i * 128, 128)
+        hid[y, :, units] = jnp.where(low, even, odd).astype(BF16)
+        for side, step in ((0, 1), (1, -1)):
+            ref = hid.at[y, :, units]
+            rc(ref, ref, es_.at[side], er.at[side], sp, tp_of(y + step, x)).start()
         return carry
 
     with jax.named_scope("expert_in"):
         lax.fori_loop(0, NTP // 2, expert_in, 0)
-    with jax.named_scope("w_fourth_dn"):
-        ring_recv(1, 3)
-    hrow = hid[...]
-
-    def expert_out(i, carry):
-        i = lax.rem(i + tp // 2, NTP // 2)
-        q = 2 * lax.rem(i, 2)
-        w = jnp.concatenate([dn[i // 2, q], dn[i // 2, q + 1]], axis=1)
-        o = dot(hrow, w).astype(BF16)
-        ob[:, :, lanes(i * 256, 256)] = o.reshape(2, CAP, 256)
-        for k in range(2):
-            j = 2 * i + k
-
-            @pl.when(j != tp)
-            def _():
-                rc(ob.at[:, :, lanes(j * COLS, COLS)], r3.at[tp], ts.at[0], tr.at[tp], sp, j).start()
-
-        return carry
-
-    with jax.named_scope("expert_out"):
-        lax.fori_loop(0, D // 256, expert_out, 0)
-
-    r3[pl.ds(tp, 1)] = ob[:, :, own].reshape(1, 2, CAP, COLS)
-
-    def give_back(i, carry):
-        c = chip_order(NZ - 1 - i)
-
-        @pl.when(c != tp)
-        def _():
-            took(r3.at[c], recv=tr.at[c])
-
+
+    def hidden_on(side, step):
+        ref = hid.at[at4(y - step), :, side * (FF // 2) : (side + 1) * (FF // 2)]
+        return rc(ref, ref, es_.at[2 + side], er.at[2], sp, tp_of(y + step, x))
+
+    def hand_over(c):
         for k in range(2):
             s = 2 * c + k
 
@@ -552,10 +528,57 @@
             def _():
                 r4[pl.ds(sp, 1)] = r3[c, pl.ds(k, 1)]
 
+    def expert_out(k):
+        h = hid[pl.ds(k, 1)].reshape(2 * CAP, FF)
+        for n in (0, 2):
+            w = jnp.concatenate([dn[n], dn[n + 1]], axis=1)
+            o = dot(h, w).astype(BF16)
+            for m in (0, 1):
+                ob[pl.ds(k, 1), n + m] = o[:, m * COLS : (m + 1) * COLS].reshape(1, 2, CAP, COLS)
+        for n in range(4):
+            to = tp_of(y, jnp.int32(n))
+
+            @pl.when(x != n)
+            def _():
+                rc(ob.at[k, n], r3.at[k * 4 + x], ts.at[0], tr.at[k * 4 + x], sp, to).start()
+
+            @pl.when(x == n)
+            def _():
+                r3[pl.ds(k * 4 + x, 1)] = ob[pl.ds(k, 1), n]
+                hand_over(k * 4 + x)
+
+    def give_back(i, carry):
+        k = i // 4
+        k = k + (k // 2) * (1 - 2 * lax.rem(k, 2))
+        c = at4(y + k) * 4 + at4(x + i)
+
+        @pl.when(lax.rem(i, 4) != 0)
+        def _():
+            took(r3.at[c], recv=tr.at[c])
+            hand_over(c)
+
         return carry
 
+    with jax.named_scope("w_second_dn"):
+        took(dn_bytes(1), recv=gr.at[9])
+    with jax.named_scope("expert_out0"):
+        expert_out(y)
+    with jax.named_scope("w_hid1"):
+        took(hid.at[0], recv=er.at[0])
+        hidden_on(0, 1).start()
+        took(hid.at[0], recv=er.at[1])
+        hidden_on(1, -1).start()
+    with jax.named_scope("expert_out1"):
+        expert_out(at4(y + 1))
+        expert_out(at4(y - 1))
+    with jax.named_scope("give_back0"):
+        lax.fori_loop(0, 4, give_back, 0)
+    with jax.named_scope("w_hid2"):
+        took(hid.at[0], recv=er.at[2])
+    with jax.named_scope("expert_out2"):
+        expert_out(at4(y + 2))
     with jax.named_scope("give_back"):
-        lax.fori_loop(0, NZ, give_back, 0)
+        lax.fori_loop(4, NZ, give_back, 0)
     sp_wait(r4, us, ur, "w_ret")
 
     results = r4[...].reshape(SLOTS, COLS)
@@ -568,17 +591,20 @@
             copy.wait_send()
 
     with jax.named_scope("sends"):
+        took(r3.at[0 : NTP - 1], send=fs.at[0])
         took(r4.at[0 : NSP - 1], send=ds_.at[0])
-        took(r3.at[0 : NTP - 1], send=ts.at[0])
+        took(r3.at[0:12], send=ts.at[0])
+        for side in (0, 1):
+            took(hid.at[0], send=es_.at[side])
+            took(hid.at[0, :, 0 : FF // 2], send=es_.at[2 + side])
         for kind, ref in enumerate((v1, v1, v1, v2, v2, v2)):
             took(ref, send=ps.at[kind])
-        for which in (0, 1):
-            for stage in range(4):
-                if which == 0 and stage == 2:
-                    for q in range(4):
-                        ring_sent(0, 2, q)
-                else:
-                    ring_sent(which, stage)
+        for stage in (0, 1, 3):
+            ring_sent(stage)
+        for q in range(4):
+            ring_sent(2, q)
+        took(dn_bytes(0), send=gs.at[8])
+        took(dn_bytes(1), send=gs.at[9])
 
 
 def per_device(
@@ -593,9 +619,19 @@
         kernel,
         name="layer",
         out_shape=jax.ShapeDtypeStruct((T, COLS), F32),
-        in_specs=[vmem] * 10 + [hbm] * 9,
+        in_specs=[hbm] * 19,
         out_specs=vmem,
         scratch_shapes=[
+            pltpu.VMEM((HEADS, T), BF16),
+            pltpu.VMEM((1, HEADS), F32),
+            pltpu.VMEM((1, HEADS), F32),
+            pltpu.VMEM((4, INNER), BF16),
+            pltpu.VMEM((4, STATE), BF16),
+            pltpu.VMEM((4, STATE), BF16),
+            pltpu.VMEM((1, INNER), F32),
+            pltpu.VMEM((1, D), F32),
+            pltpu.VMEM((2, T), jnp.int32),
+            pltpu.VMEM((2, T), F32),
             pltpu.VMEM((T, INNER), BF16),
             pltpu.VMEM((T, INNER), BF16),
             pltpu.VMEM((T, STATE), BF16),
@@ -622,8 +658,6 @@
             pltpu.VMEM((2, 2, T // 2, COLS), BF16),
             pltpu.VMEM((2, 2, T // 4, COLS), BF16),
             pltpu.VMEM((T, COLS), F32),
-            pltpu.VMEM((8, T), F32),
-            pltpu.VMEM((NTP, 8, T), F32),
             pltpu.VMEM((T, COLS), BF16),
             pltpu.VMEM((SLOTS, T), BF16),
             pltpu.VMEM((T, SLOTS), BF16),
@@ -631,10 +665,11 @@
             pltpu.VMEM((NSP, CAP, COLS), BF16),
             pltpu.VMEM((NSP, CAP, COLS), BF16),
             pltpu.VMEM((2, CAP, D), BF16),
+            pltpu.VMEM((2 * CAP, D), BF16),
             pltpu.VMEM((4, 4, COLS, D), BF16),
-            pltpu.VMEM((4, 4, FF, COLS), BF16),
-            pltpu.VMEM((2 * CAP, FF), BF16),
-            pltpu.VMEM((2, CAP, D), BF16),
+            pltpu.VMEM((4, FF, COLS), BF16),
+            pltpu.VMEM((4, 2 * CAP, FF), BF16),
+            pltpu.VMEM((4, 4, 2, CAP, COLS), BF16),
             pltpu.VMEM((NTP, 2, CAP, COLS), BF16),
             pltpu.VMEM((NSP, CAP, COLS), BF16),
             dma((3,)), dma((3,)),
@@ -642,13 +677,13 @@
             dma((1,)), dma((1,)),
             dma((1,)), dma((1,)),
             dma((6,)), dma((6,)),
-            dma((1,)), dma((1,)),
             dma((1,)), dma((NZ,)),
             dma((1,)), dma((1,)),
             dma((1,)), dma((NTP,)),
             dma((1,)), dma((1,)),
-            dma((12,)), dma((12,)),
-            dma((9,)),
+            dma((4,)), dma((3,)),
+            dma((10,)), dma((10,)),
+            dma((19,)),
         ],
         compiler_params=pltpu.CompilerParams(
             collective_id=0, has_side_effects=True, vmem_limit_bytes=60 * 1024 * 1024

time: 126 us -> 115 us (0.913)
  Pallas kernels: 124 us -> 113 us
    pallas_call x1, Pallas kernels: 124 us -> 113 us  [per_device(): pl.pallas_call(kernel, name='layer', out_shape=jax.ShapeDtypeStruct((T, C...]
where the time goes in v3:
time: 115 us
  Pallas kernels  113 us (98%)
  other arithmetic  1.58 us (1%)
    pallas_call x1, Pallas kernels, per_device(): pl.pallas_call(kernel, name='layer', out_shape=jax.ShapeDtypeStruct((T, C...  113 us

profile of v3, /device:TPU:1, one launch (start us, length us, event | category | flops | bytes accessed | tf_op | source)
XLA Modules:
  0.0 114.6 jit_solution(2038953868264062697)
XLA Ops:
  0.0 113.0 %layer.1 = f32[384,128]{1,0:T(8,128)} custom-call(bf16[4,384]{1,0:T(4,128)(2,1)} %bitcast.24, f32[1,4]{1,0:T(1,128)} %bitcast.30, f32[1,4]{1,0:T(1,128)} %bitcast.31, bf16[4,256]{1,0:T(4,128)(2,1)} %tap_xh.1, bf16[4,128]{1,0:T(4,128)(2,1)} %bitcast.27, bf16[4,128]{1,0:T(4,128)(2,1)} %bitcast.28, f32[1,256]{1,0:T(1,128)} %bitcast.29, f32[1,2048]{1,0:T(1,128)} %bitcast.23, ...), custom_call_target="tpu_custom_call" | custom-call | tf_op jit(solution)/shard_map/layer/pallas_call | solution.py:618
  113.0 1.6 %convert_element_type.3 = bf16[384,128]{1,0:T(8,128)(2,1)} convert(f32[384,128]{1,0:T(8,128)} %layer.1) | non-fusion elementwise | flops 49152 | bytes 294912 | tf_op jit(solution)/shard_map/convert_element_type | solution.py:697

commit v4 on v3

--- a/solution.py
+++ b/solution.py
@@ -139,27 +139,27 @@
     def neighbour(axis, step):
         return tp_of(y, x + step) if axis == 0 else tp_of(y + step, x)
 
-    QN = COLS // 2
+    WIDE = ((0, 1152), (1152, 896))
+    PIECES = (((0, 384), (384, 384), (768, 384)), ((1152, 256), (1408, 256), (1664, 384)))
 
     def at4(v):
         return lax.rem(v + 4, 4)
 
     def ring(axis, stage, quarter=None, piece=None):
-        base = axis * QN
+        wide = pl.ds(*(WIDE[axis] if piece is None else PIECES[axis][piece]))
         copies = []
         for side, step in ((0, 1), (1, -1)):
             k = stage if quarter is None else 4 + quarter
-            part = pl.ds(*((base + side * (QN // 2), QN // 2) if stage % 2 else (base, QN)))
+            part = pl.ds(side * (COLS // 2), COLS // 2) if stage % 2 else pl.ds(0, COLS)
             if quarter is not None:
-                part = pl.ds(base + quarter * (QN // 4), QN // 4)
+                part = pl.ds(quarter * (COLS // 4), COLS // 4)
             back = step if stage % 2 else 0
             if stage < 2:
                 to = neighbour(axis, step)
                 oy, ox = (y, at4(x - back)) if axis == 0 else (at4(y - back), x)
-                ref = gu.at[oy, ox, part]
+                ref = gu.at[oy, ox, part, wide]
             else:
                 to = neighbour(1 - axis, step)
-                wide = slice(None) if piece is None else pl.ds(piece * (D // 4), D // 4)
                 if axis == 0:
                     ref = gu.at[at4(y - back), :, part, wide]
                 else:
@@ -179,10 +179,10 @@
         return [c for axis in (0, 1) for c in ring(axis, stage, quarter, piece)]
 
     def ring_bytes(stage, quarter=None):
-        rows_ = (QN // 2 if stage % 2 else QN) if quarter is None else QN // 4
         if stage < 2:
-            return gu.at[0, :, pl.ds(0, rows_)]
-        return gu.at[:, :, pl.ds(0, rows_)]
+            return gu.at[0, 0 : 2 - stage]
+        rows_ = COLS // 2 if quarter is None else COLS // 4
+        return gu.at[0:2, :, pl.ds(0, rows_)]
 
     def ring_recv(stage, quarter=None):
         took(ring_bytes(stage, quarter), recv=gr.at[stage if quarter is None else 4 + quarter])
@@ -422,11 +422,8 @@
         here = s1[h, pl.ds(at4(p2 + step), 1), side * PART : (side + 1) * PART].reshape(PART, COLS)
         z2[h, side] = (here.astype(F32) + v2[h, side].astype(F32)).astype(BF16)
         sum2[n].start()
-    start(rings(2, 1, 3))
     start(rings(2, 2))
     start(rings(2, 3))
-    took(dn_bytes(0), recv=gr.at[8])
-    start(ring_dn(1))
     halves = []
     for h in (0, 1):
         p, p2 = place(h)
@@ -485,6 +482,8 @@
     start(rings(3))
     with jax.named_scope("forward"):
         lax.fori_loop(0, NZ, forward, 0)
+    took(dn_bytes(0), recv=gr.at[8])
+    start(ring_dn(1))
     with jax.named_scope("w_fwd"):
         took(r3.at[0 : NTP - 1], recv=fr.at[0])
     xf = xb[...].reshape(2 * CAP, D).astype(F32)

time: 115 us -> 114 us (level)
  the two profiles are of different devices: /device:TPU:1 before, /device:TPU:21 now
where the time goes in v4:
time: 114 us
  Pallas kernels  113 us (99%)
  other arithmetic  1.58 us (1%)
    pallas_call x1, Pallas kernels, per_device(): pl.pallas_call(kernel, name='layer', out_shape=jax.ShapeDtypeStruct((T, C...  113 us

profile of v4, /device:TPU:21, one launch (start us, length us, event | category | flops | bytes accessed | tf_op | source)
XLA Modules:
  0.0 114.2 jit_solution(14326403033339479192)
XLA Ops:
  0.0 112.6 %layer.1 = f32[384,128]{1,0:T(8,128)} custom-call(bf16[4,384]{1,0:T(4,128)(2,1)} %bitcast.24, f32[1,4]{1,0:T(1,128)} %bitcast.30, f32[1,4]{1,0:T(1,128)} %bitcast.31, bf16[4,256]{1,0:T(4,128)(2,1)} %tap_xh.1, bf16[4,128]{1,0:T(4,128)(2,1)} %bitcast.27, bf16[4,128]{1,0:T(4,128)(2,1)} %bitcast.28, f32[1,256]{1,0:T(1,128)} %bitcast.29, f32[1,2048]{1,0:T(1,128)} %bitcast.23, ...), custom_call_target="tpu_custom_call" | custom-call | tf_op jit(solution)/shard_map/layer/pallas_call | solution.py:617
  112.6 1.6 %convert_element_type.3 = bf16[384,128]{1,0:T(8,128)(2,1)} convert(f32[384,128]{1,0:T(8,128)} %layer.1) | non-fusion elementwise | flops 49152 | bytes 294912 | tf_op jit(solution)/shard_map/convert_element_type | solution.py:696
